TPU v7x, 32 devices: a whole 2x2x4 slice. The times are simulated.
32 devices in a mesh: ep: 8 (over z, x), tp: 4 (over y, core).
Axes of the slice: x: 2, y: 2, z: 4, core: 2. Of those that a mesh axis runs over, the one named last changes fastest.
Arguments:
- queries: bfloat16 [2048, 8, 128], P('ep', 'tp'), may hold values from -256 to 256
- keys: bfloat16 [2048, 4, 128], P('ep', 'tp'), may hold values from -8 to 8
- values: bfloat16 [2048, 4, 128], P('ep', 'tp'), may hold values from -6 to 6
- attn_lambda: float32 [8], P('tp'), may hold values from 0.3 to 0.8
- head_gain: float32 [128], replicated, may hold values from 0.1 to 1.9
- w_out: bfloat16 [1024, 2048], replicated, may hold values from -0.1875 to 0.1875
- moe_rows: bfloat16 [4096, 2048], P('ep'), may hold values from -6 to 6
- moe_gain: float32 [2048], replicated, may hold values from 0.1 to 1.9
- routes: int32 [4096, 2], P('ep'), may hold values from 0 to 7, all different within a row; in each aligned block of 128 rows (0 to 127, 128 to 255, ...) at most 64 rows name the same one
- route_weights: float32 [4096, 2], P('ep'), may hold values from 0.1 to 1
- w_gate: bfloat16 [8, 2048, 1024], P('ep', None, 'tp'), may hold values from -0.125 to 0.125
- w_up: bfloat16 [8, 2048, 1024], P('ep', None, 'tp'), may hold values from -0.125 to 0.125
- w_down: bfloat16 [8, 1024, 2048], P('ep', 'tp'), may hold values from -0.1875 to 0.1875
Outputs:
- mixer_out: bfloat16 [2048, 2048], P(('ep', 'tp'))
- moe_out: bfloat16 [4096, 2048], P(('ep', 'tp'))
Inputs may be any that keep to these rules, and one draw needn't show every extreme that they name: `routes`: each row names 2 different experts. In each aligned block of 128 rows (the rows of moe_out that one device holds) no expert is named by more than 64 rows, a bound that some block reaches.
All inputs are finite; a program needn't handle non-finite values.
Results may differ from a plain program's by a relative error of at most 0.011.
Values may be sent and summed in bfloat16 or wider, within the bound.
A program may use at most 128 MiB of HBM per device.

v0:
```python
import jax
import jax.numpy as jnp
from jax import lax
from jax.sharding import PartitionSpec as P

EPSILON = 1e-06
MASKED = -1e30


def rms_scaled(values_f, gain):
    mean_sq = jnp.mean(values_f * values_f, axis=-1, keepdims=True)
    return values_f * lax.rsqrt(mean_sq + EPSILON) * gain


def slot_numbers(block_routes, experts):
    flat_ids = block_routes.reshape(-1)
    matches = (flat_ids[:, None] == lax.iota(jnp.int32, experts)[None, :]).astype(jnp.int32)
    earlier = jnp.cumsum(matches, axis=0) - matches
    return jnp.sum(earlier * matches, axis=1).reshape(block_routes.shape)


def fill_slots(block_rows, block_routes, experts, capacity):
    slot_ids = slot_numbers(block_routes, experts)
    model_width = block_rows.shape[1]
    copies = jnp.broadcast_to(block_rows[:, None, :], block_routes.shape + (model_width,))
    blank_slots = jnp.zeros((experts, capacity, model_width), block_rows.dtype)
    return (blank_slots.at[block_routes, slot_ids].set(copies), slot_ids)


def local(
    queries,
    keys,
    values,
    attn_lambda,
    head_gain,
    w_out,
    moe_rows,
    moe_gain,
    routes,
    route_weights,
    w_gate,
    w_up,
    w_down,
):
    positions = queries.shape[0]
    q_heads = queries.shape[1]
    kv_heads = keys.shape[1]
    head_dim = queries.shape[2] // 2
    value_dim = values.shape[2]
    per_key = q_heads // kv_heads
    first_pos = lax.axis_index("ep") * positions
    query_pos = first_pos + lax.iota(jnp.int32, positions)
    last_pos = first_pos + positions - 1
    query_view = queries.reshape(positions, kv_heads, per_key, 2, head_dim)
    inv_scale = head_dim ** (-0.5)
    start_max = jnp.full((positions, kv_heads, per_key, 2), MASKED, jnp.float32)
    start_total = jnp.zeros((positions, kv_heads, per_key, 2), jnp.float32)
    start_acc = jnp.zeros((positions, kv_heads, per_key, 2, value_dim), jnp.float32)
    carry = (start_max, start_total, start_acc)
    key_piece = lax.all_gather(keys, "ep", axis=0, tiled=True)
    value_piece = lax.all_gather(values, "ep", axis=0, tiled=True)
    shard_count = key_piece.shape[0] // positions
    together = 1
    for candidate in (2, 3, 4):
        if shard_count % candidate == 0:
            together = candidate
    block_len = together * positions
    blocks = shard_count // together
    key_blocks = key_piece.reshape(blocks, block_len, kv_heads, 2, head_dim)
    value_blocks = value_piece.reshape(blocks, block_len, kv_heads, value_dim)
    block_starts = block_len * lax.iota(jnp.int32, blocks)

    def visit(running, inputs):
        key_blk, value_blk, block_start = inputs

        def update(current):
            run_max, run_total, run_acc = current
            key_pos = block_start + lax.iota(jnp.int32, block_len)
            scores = (
                jnp.einsum(
                    "qkgmd,pkmd->qkgmp", query_view, key_blk, preferred_element_type=jnp.float32
                )
                * inv_scale
            )
            allowed = key_pos[None, :] <= query_pos[:, None]
            scores = jnp.where(allowed[:, None, None, None, :], scores, MASKED)
            new_max = jnp.maximum(run_max, jnp.max(scores, axis=-1))
            shrink = jnp.exp(run_max - new_max)
            weights = jnp.exp(scores - new_max[..., None])
            run_total = run_total * shrink + jnp.sum(weights, axis=-1)
            run_acc = run_acc * shrink[..., None] + jnp.einsum(
                "qkgmp,pkv->qkgmv",
                weights.astype(jnp.bfloat16),
                value_blk,
                preferred_element_type=jnp.float32,
            )
            return (new_max, run_total, run_acc)

        def keep(current):
            return current

        return (lax.cond(block_start <= last_pos, update, keep, running), None)

    carry, unused = lax.scan(visit, carry, (key_blocks, value_blocks, block_starts))
    run_max, run_total, run_acc = carry
    ratios = run_acc / run_total[..., None]
    lambda_view = attn_lambda.reshape(1, kv_heads, per_key, 1)
    head_out = ratios[:, :, :, 0] - lambda_view * ratios[:, :, :, 1]
    attn_rows = (
        rms_scaled(head_out, head_gain).astype(jnp.bfloat16).reshape(positions, q_heads * value_dim)
    )
    tp_count = lax.axis_size("tp")
    tp_id = lax.axis_index("tp")
    exchanged = lax.all_to_all(
        attn_rows.reshape(positions, q_heads, value_dim),
        "tp",
        split_axis=0,
        concat_axis=1,
        tiled=True,
    )
    mixer_out = jnp.dot(
        exchanged.reshape(positions // tp_count, tp_count * q_heads * value_dim),
        w_out,
        preferred_element_type=jnp.float32,
    ).astype(jnp.bfloat16)
    experts = lax.axis_size("ep")
    dev_rows = moe_rows.shape[0] // tp_count
    top_count = routes.shape[1]
    capacity = max(2, 2 * dev_rows * top_count // experts)
    model_width = moe_rows.shape[1]
    hidden_units = w_gate.shape[2]
    own_routes = lax.dynamic_slice_in_dim(routes, tp_id * dev_rows, dev_rows, 0)
    own_weights = lax.dynamic_slice_in_dim(route_weights, tp_id * dev_rows, dev_rows, 0)
    own_rows = rms_scaled(
        lax.dynamic_slice_in_dim(moe_rows, tp_id * dev_rows, dev_rows, 0).astype(jnp.float32),
        moe_gain,
    ).astype(jnp.bfloat16)
    outgoing, own_slots = fill_slots(own_rows, own_routes, experts, capacity)
    arrived = lax.all_to_all(outgoing, "ep", split_axis=0, concat_axis=0, tiled=True)
    slot_rows = lax.all_gather(arrived[None], "tp", axis=0, tiled=True)
    flat_rows = slot_rows.reshape(-1, model_width)
    gate_out = jnp.dot(flat_rows, w_gate[0], preferred_element_type=jnp.float32)
    up_out = jnp.dot(flat_rows, w_up[0], preferred_element_type=jnp.float32)
    hidden = (
        (jax.nn.silu(gate_out) * up_out)
        .astype(jnp.bfloat16)
        .reshape(slot_rows.shape[:-1] + (hidden_units,))
    )
    flat_terms = hidden.reshape(-1, hidden_units)
    summed = lax.psum_scatter(
        jnp.dot(flat_terms, w_down[0], preferred_element_type=jnp.float32)
        .reshape(hidden.shape[:-1] + (model_width,))
        .astype(jnp.bfloat16),
        "tp",
        scatter_dimension=0,
        tiled=True,
    )
    returned = lax.all_to_all(summed, "ep", split_axis=1, concat_axis=1, tiled=True)[0]
    picked = returned[own_routes, own_slots]
    moe_out = jnp.sum(own_weights[..., None] * picked.astype(jnp.float32), axis=1).astype(
        jnp.bfloat16
    )
    return (mixer_out, moe_out)


def solution(mesh):
    return jax.shard_map(
        local,
        mesh=mesh,
        in_specs=(
            P("ep", "tp", None),
            P("ep", "tp", None),
            P("ep", "tp", None),
            P("tp"),
            P(),
            P(),
            P("ep", None),
            P(),
            P("ep", None),
            P("ep", None),
            P("ep", None, "tp"),
            P("ep", None, "tp"),
            P("ep", "tp", None),
        ),
        out_specs=(P(("ep", "tp"), None), P(("ep", "tp"), None)),
        check_vma=False,
    )
```

profile of v0, /device:TPU:16, one launch (start us, length us, event | category | flops | bytes accessed | tf_op | source)
XLA Modules:
  0.0 325.6 jit_solution(4695768976303798606)
XLA Ops:
  7.2 0.8 constant_dynamic-slice_fusion
  8.4 0.6 reduce-window.6
  9.7 1.2 fusion.24
  10.9 1.3 fusion.26
  12.2 0.6 broadcast_in_dim.60
  12.8 1.2 reshape.233
  14.3 33.4 %scatter_fusion = bf16[8,64,2048]{2,1,0:T(8,128)(2,1)S(1)} fusion(bf16[8,64,2048]{2,1,0:T(8,128)(2,1)S(1)} %broadcast_in_dim.58, s32[256]{0:T(256)S(1)} %reshape.231, bf16[256,2048]{1,0:T(8,128)(2,1)} %reshape.233), kind=kCustom, calls=%fused_computation.1 | custom fusion | bytes 3147776 | tf_op jit(solution)/shard_map/scatter | solution.py:27
  47.7 52.4 %all_to_all.25 = bf16[8,64,2048]{2,1,0:T(8,128)(2,1)} all-to-all(bf16[8,64,2048]{2,1,0:T(8,128)(2,1)S(1)} %scatter_fusion), channel_id=1, replica_groups=mesh['ep'=8,'tp'=4] {'ep'}, dimensions={0} | all-to-all | bytes 4194304 | tf_op jit(solution)/shard_map/all_to_all | solution.py:139
  100.2 58.7 %all-gather.3.cloned.1.call-done = bf16[32,64,2048]{2,1,0:T(8,128)(2,1)} async-done(((bf16[8,64,2048]{2,1,0:T(8,128)(2,1)}), bf16[32,64,2048]{2,1,0:T(8,128)(2,1)}) %all-gather.3.cloned.1.call-update) | async-done | bytes 8388624 | tf_op jit(solution)/shard_map/all_gather | solution.py:140
  158.9 5.9 %fusion.29 = f32[2048,256]{1,0:T(8,128)S(1)} fusion(bf16[2048,2048]{1,0:T(8,128)(2,1)} %bitcast.134, bf16[1,2048,256]{2,1,0:T(8,128)(2,1)S(1)} %copy-done.7), kind=kOutput, calls=%fused_computation.40 | convolution fusion | flops 2147483648 | bytes 11534336 | tf_op jit(solution)/shard_map/dot_general | solution.py:142
  164.9 2.6 fusion.23
  167.6 5.6 %convolution_convert_fusion = bf16[4,8,64,2048]{3,2,1,0:T(8,128)(2,1)} fusion(bf16[4,8,64,256]{3,2,1,0:T(8,128)(2,1)S(1)} %bitcast.130, bf16[1,256,2048]{2,1,0:T(8,128)(2,1)S(1)} %copy-done), kind=kOutput, calls=%fused_computation.28 | convolution fusion | flops 2151677952 | bytes 10485760 | tf_op jit(solution)/shard_map/dot_general | solution.py:151
  173.2 0.8 copy-done.2
  174.0 27.0 %all_gather.9 = bf16[2048,1,128]{2,0,1:T(8,128)(2,1)S(1)} all-gather(bf16[256,1,128]{2,0,1:T(8,128)(2,1)S(1)} %copy-done.2), channel_id=1, replica_groups=mesh['ep'=8,'tp'=4] {'ep'}, dimensions={0}, use_global_device_ids=true | all-gather | bytes 589824 | tf_op jit(solution)/shard_map/all_gather | solution.py:60
  201.3 0.7 copy.64
  202.1 31.4 %all_gather.10 = bf16[2048,1,128]{2,0,1:T(8,128)(2,1)S(1)} all-gather(bf16[256,1,128]{2,0,1:T(8,128)(2,1)S(1)} %copy-done.3), channel_id=1, replica_groups=mesh['ep'=8,'tp'=4] {'ep'}, dimensions={0}, use_global_device_ids=true | all-gather | bytes 589824 | tf_op jit(solution)/shard_map/all_gather | solution.py:61
  234.0 8.8 %while.15 = (s32[]{:T(128)}, f32[256,1,2,2]{0,2,3,1:T(2,128)S(1)}, f32[256,1,2,2]{0,2,3,1:T(2,128)S(1)}, f32[256,1,2,2,128]{0,4,3,2,1:T(8,128)S(1)}, s32[2]{0:T(...) while((s32[]{:T(128)}, f32[256,1,2,2]{0,2,3,1:T(2,128)S(1)}, ...), condition=%wide.region_5.6_spmd.clone, body=%wide.region_0.5_spmd.clone.sunk | while | flops 411570432 | bytes 15155487 | solution.py:104
  235.1 3.3 %conditional.3 = ((f32[256,1,2,2]{0,2,3,1:T(2,128)S(1)}, f32[256,1,2,2]{0,2,3,1:T(2,128)S(1)}, f32[256,1,2,2,128]{0,4,3,2,1:T(8,128)S(1)})) conditional(s32[]{:T(128)} %convert_element_type.73, (f32[256,1,2,2]{0,2,3,1:T(2,128)S(1)}, f32[256,1,2,2]{0,2,3,1:T(2,128)S(1)}, f32[256,1,2,2,128]{0,4,3,2,1:T(8,128)S(1)}) %tuple.48, (s32[]{:T(128)}, ...), branch_computations={%region_1.1_spmd, %region_2.4_spmd} | conditional | flops 411570432 | bytes 15154224 | solution.py:102
  235.9 0.9 fusion.4
  236.8 1.0 fusion.5
  239.5 3.3 %conditional.3 = ((f32[256,1,2,2]{0,2,3,1:T(2,128)S(1)}, f32[256,1,2,2]{0,2,3,1:T(2,128)S(1)}, f32[256,1,2,2,128]{0,4,3,2,1:T(8,128)S(1)})) conditional(s32[]{:T(128)} %convert_element_type.73, (f32[256,1,2,2]{0,2,3,1:T(2,128)S(1)}, f32[256,1,2,2]{0,2,3,1:T(2,128)S(1)}, f32[256,1,2,2,128]{0,4,3,2,1:T(8,128)S(1)}) %tuple.48, (s32[]{:T(128)}, ...), branch_computations={%region_1.1_spmd, %region_2.4_spmd} | conditional | flops 411570432 | bytes 15154224 | solution.py:102
  240.3 0.9 fusion.4
  241.2 1.0 fusion.5
  243.2 0.7 broadcast_divide_fusion
  244.9 7.0 %all_to_all.26 = bf16[256,2,128]{2,1,0:T(2,128)(2,1)S(1)} all-to-all(bf16[256,2,128]{2,1,0:T(2,128)(2,1)S(1)} %fusion.37), channel_id=1, replica_groups=mesh['ep'=8,'tp'=4] {'tp'}, dimensions={0} | all-to-all | bytes 262144 | tf_op jit(solution)/shard_map/all_to_all | solution.py:114
  251.9 10.7 %all-to-all-start.2 = ((bf16[1,8,64,2048]{3,2,0,1:T(8,128)(2,1)}), bf16[1,8,64,2048]{3,2,0,1:T(8,128)(2,1)S(1)}, u32[]{:S(2)}, u32[]{:S(2)}) async-start(bf16[1,8,64,2048]{3,2,0,1:T(8,128)(2,1)} %bitcast.127), calls=%async_computation.3 | async-start | bytes 4194304 | tf_op jit(solution)/shard_map/all_to_all | solution.py:158
  262.7 0.7 constant_dynamic-slice_fusion.1
  263.7 3.7 %convolution_convert_fusion.1 = bf16[64,2048]{1,0:T(8,128)(2,1)} fusion(bf16[64,1024]{1,0:T(8,128)(2,1)S(1)} %reshape.221, bf16[1024,2048]{1,0:T(8,128)(2,1)} %param.22), kind=kOutput, calls=%fused_computation.31 | convolution fusion | flops 268566528 | bytes 4587520 | tf_op jit(solution)/shard_map/dot_general | solution.py:121
  267.5 39.7 %all-to-all-done.2 = bf16[1,8,64,2048]{3,2,0,1:T(8,128)(2,1)S(1)} async-done(((bf16[1,8,64,2048]{3,2,0,1:T(8,128)(2,1)}), bf16[1,8,64,2048]{3,2,0,1:T(8,128)(2,1)S(1)}, u32[]{:S(2)}, u32[]{:S(2)}) %all-to-all-start.2) | async-done | bytes 2097184 | tf_op jit(solution)/shard_map/all_to_all | solution.py:158
  307.2 5.3 %gather_fusion = bf16[256,2048]{1,0:T(8,128)(2,1)} fusion(bf16[8,64,2048]{2,1,0:T(8,128)(2,1)S(1)} %bitcast.126, s32[256]{0:T(256)S(1)} %reshape.225), kind=kCustom, calls=%fused_computation | custom fusion | bytes 2099200 | tf_op jit(solution)/shard_map/gather | solution.py:159
  312.5 2.4 reshape.239
  314.9 3.9 %multiply_reduce_fusion = bf16[128,2048]{1,0:T(8,128)(2,1)} fusion(f32[128,2,2048]{2,1,0:T(2,128)S(1)} %reshape.239, f32[128,2]{1,0:T(8,128)S(1)} %copy.73), kind=kLoop, calls=%fused_computation.32 | loop fusion | flops 786432 | bytes 2622464 | tf_op jit(solution)/shard_map/reduce_sum | solution.py:160
  (73 shorter events, 7.9 us)
Async XLA Ops:
  7.2 160.4 %copy-start = (bf16[1,256,2048]{2,1,0:T(8,128)(2,1)S(1)}, bf16[1,256,2048]{2,1,0:T(8,128)(2,1)}, u32[]{:S(2)}) copy-start(bf16[1,256,2048]{2,1,0:T(8,128)(2,1)} %param.29) | copy-start | bytes 3145732
  7.2 151.7 %all-gather.3.cloned.1.call-start = ((), (), s32[]{:S(2)}) async-start(), calls=%async_computation.5 | async-start | bytes 10485760 | tf_op jit(solution)/shard_map/all_gather | solution.py:140
  100.1 58.8 %copy-start.7 = (bf16[1,2048,256]{2,1,0:T(8,128)(2,1)S(1)}, bf16[1,2048,256]{2,1,0:T(8,128)(2,1)}, u32[]{:S(2)}) copy-start(bf16[1,2048,256]{2,1,0:T(8,128)(2,1)} %param.27) | copy-start | bytes 3145732
  100.1 151.7 %reduce-scatter.2.cloned.1.call-start = ((), (), s32[]{:S(2)}) async-start(), calls=%async_computation.4 | async-start | bytes 10485760 | tf_op jit(solution)/shard_map/reduce_scatter | solution.py:150
  158.9 5.9 %copy-start.6 = (bf16[32,64,2048]{2,1,0:T(8,128)(2,1)S(1)}, bf16[32,64,2048]{2,1,0:T(8,128)(2,1)}, u32[]{:S(2)}) copy-start(bf16[32,64,2048]{2,1,0:T(8,128)(2,1)} %all-gather.3.cloned.1.call-done) | copy-start | bytes 25165828
  158.9 6.0 %copy-start.8 = (bf16[1,2048,256]{2,1,0:T(8,128)(2,1)S(1)}, bf16[1,2048,256]{2,1,0:T(8,128)(2,1)}, u32[]{:S(2)}) copy-start(bf16[1,2048,256]{2,1,0:T(8,128)(2,1)} %param.28) | copy-start | bytes 3145732
  173.1 0.8 copy-start.2
  173.2 28.9 %copy-start.3 = (bf16[256,1,128]{2,0,1:T(8,128)(2,1)S(1)}, bf16[256,1,128]{2,0,1:T(8,128)(2,1)}, u32[]{:S(2)}) copy-start(bf16[256,1,128]{2,0,1:T(8,128)(2,1)} %param.19) | copy-start | bytes 196612
  200.9 32.8 %copy-start.1 = (bf16[256,2,128]{2,1,0:T(2,128)(2,1)S(1)}, bf16[256,2,128]{2,1,0:T(2,128)(2,1)}, u32[]{:S(2)}) copy-start(bf16[256,2,128]{2,1,0:T(2,128)(2,1)} %param.17) | copy-start | bytes 393220
  242.8 1.1 copy-start.4
  242.8 1.6 copy-start.5
  251.9 55.3 %all-to-all-start.2 = ((bf16[1,8,64,2048]{3,2,0,1:T(8,128)(2,1)}), bf16[1,8,64,2048]{3,2,0,1:T(8,128)(2,1)S(1)}, u32[]{:S(2)}, u32[]{:S(2)}) async-start(bf16[1,8,64,2048]{3,2,0,1:T(8,128)(2,1)} %bitcast.127), calls=%async_computation.3 | async-start | bytes 4194304 | tf_op jit(solution)/shard_map/all_to_all | solution.py:158
Sparse Core Ops, SparseCore 0:
  100.2 58.6 all-gather.2
  173.3 71.4 reduce-scatter.1
where the time goes:
time: 331 us; the launch traced here: 326 us
  blocking collectives  118 us (36%)
  waiting for transfers between devices  98.5 us (30%)
  local copies, waits for them, and re-layouts  49.9 us (15%)
  matrix products  20.7 us (6%)
  between operations  14.4 us (4%)
  other arithmetic  12.3 us (4%)
  starting transfers between devices  10.8 us (3%)
    all_gather x1, waiting for transfers between devices, local(): slot_rows = lax.all_gather(arrived[None], 'tp', axis=0, tiled=True)  58.7 us
    all_to_all x1, blocking collectives, local(): lax.all_to_all(outgoing, 'ep', split_axis=0, concat_axis=0, tiled=True)  52.4 us
    all_to_all x1, waiting for transfers between devices, local(): lax.all_to_all(summed, 'ep', split_axis=1, concat_axis=1, tiled=True)[0]  39.7 us
    scatter x1, local copies, waits for them, and re-layouts, fill_slots(): return (blank_slots.at[block_routes, slot_ids].set(copies), slot_ids)  33.4 us
    all_gather x1, blocking collectives, local(): value_piece = lax.all_gather(values, 'ep', axis=0, tiled=True)  31.4 us
    all_gather x1, blocking collectives, local(): key_piece = lax.all_gather(keys, 'ep', axis=0, tiled=True)  27 us
    all_to_all x1, starting transfers between devices, local(): lax.all_to_all(summed, 'ep', split_axis=1, concat_axis=1, tiled=True)[0]  10.7 us
    all_to_all x1, blocking collectives, local(): lax.all_to_all(attn_rows.reshape(positions, q_heads, value_dim), 'tp', sp...  6.99 us
  transfers between devices with their start and end apart: 3, of which 2 were waited for; matrix products, arithmetic and copies ran while one was open for 5% of the time, Pallas kernels for 0%

commit v1 on v0

--- a/solution.py
+++ b/solution.py
@@ -1,6 +1,10 @@
+import functools
+
 import jax
 import jax.numpy as jnp
 from jax import lax
+from jax.experimental import pallas as pl
+from jax.experimental.pallas import tpu as pltpu
 from jax.sharding import PartitionSpec as P
 
 EPSILON = 1e-06
@@ -12,19 +16,329 @@
     return values_f * lax.rsqrt(mean_sq + EPSILON) * gain
 
 
-def slot_numbers(block_routes, experts):
-    flat_ids = block_routes.reshape(-1)
-    matches = (flat_ids[:, None] == lax.iota(jnp.int32, experts)[None, :]).astype(jnp.int32)
-    earlier = jnp.cumsum(matches, axis=0) - matches
-    return jnp.sum(earlier * matches, axis=1).reshape(block_routes.shape)
-
-
-def fill_slots(block_rows, block_routes, experts, capacity):
-    slot_ids = slot_numbers(block_routes, experts)
-    model_width = block_rows.shape[1]
-    copies = jnp.broadcast_to(block_rows[:, None, :], block_routes.shape + (model_width,))
-    blank_slots = jnp.zeros((experts, capacity, model_width), block_rows.dtype)
-    return (blank_slots.at[block_routes, slot_ids].set(copies), slot_ids)
+def expert_kernel(
+    n,
+    out_ref,
+    mine_ref,
+    gate_ref,
+    up_ref,
+    down_ref,
+    mix_ref,
+    res_ref,
+    slots,
+    part,
+    pair_in,
+    col_in,
+    back,
+    hidden_ref,
+    acc,
+    send_a,
+    recv_a,
+    send_y,
+    recv_y,
+    send_c,
+    recv_c,
+    send_b,
+    recv_b,
+    send_p,
+    recv_p,
+    send_q,
+    recv_q,
+    send_r,
+    recv_r,
+    local_sem,
+):
+    me = lax.axis_index("ep")
+    tp = lax.axis_index("tp")
+    row = tp // 2
+    col = tp % 2
+    other_row = 1 - row
+    other_col = 1 - col
+    pair_peer = row * 2 + other_col
+    row_peer = other_row * 2 + col
+    own_blk = col * 2 + row
+    far_blk = col * 2 + other_row
+    slot_count = slots.shape[2]
+    width = slots.shape[3]
+
+    def remote(src, dst, ssem, rsem, ep_id, tp_id):
+        return pltpu.make_async_remote_copy(
+            src_ref=src,
+            dst_ref=dst,
+            send_sem=ssem,
+            recv_sem=rsem,
+            device_id=(ep_id, tp_id),
+            device_id_type=pl.DeviceIdType.MESH,
+        )
+
+    barrier = pltpu.get_barrier_semaphore()
+
+    @pl.loop(1, n)
+    def _(d):
+        pl.semaphore_signal(
+            barrier, inc=1, device_id=((me + d) % n, tp), device_id_type=pl.DeviceIdType.MESH
+        )
+
+    for peer in (pair_peer, row_peer):
+        pl.semaphore_signal(
+            barrier, inc=1, device_id=(me, peer), device_id_type=pl.DeviceIdType.MESH
+        )
+    fills = [
+        pltpu.make_async_copy(
+            mine_ref.at[b], slots.at[0, (b % 2) * 2 + b // 2], local_sem.at[b]
+        )
+        for b in range(4)
+    ]
+    for fill in fills:
+        fill.start()
+    pl.semaphore_wait(barrier, n + 1)
+
+    def copy_a(d):
+        return remote(
+            out_ref.at[d], slots.at[d, own_blk], send_a.at[d], recv_a.at[d], (me + d) % n, tp
+        )
+
+    def copy_y(d):
+        block = slots.at[d, own_blk]
+        return remote(block, block, send_y.at[d], recv_y.at[d], me, row_peer)
+
+    def copy_c(d):
+        block = slots.at[d, own_blk]
+        return remote(block, block, send_c.at[d], recv_c.at[d], me, pair_peer)
+
+    def copy_b(d):
+        block = slots.at[d, far_blk]
+        return remote(block, block, send_b.at[d], recv_b.at[d], me, pair_peer)
+
+    def copy_p(d):
+        return remote(
+            part.at[d, pl.ds(other_col * 2, 2)],
+            pair_in.at[d],
+            send_p.at[d],
+            recv_p.at[d],
+            me,
+            pair_peer,
+        )
+
+    def copy_q(d):
+        return remote(part.at[d, far_blk], col_in.at[d], send_q.at[d], recv_q.at[d], me, row_peer)
+
+    def copy_r(d):
+        return remote(
+            part.at[d, own_blk], back.at[d], send_r.at[d], recv_r.at[d], (me + n - d) % n, tp
+        )
+
+    @pl.loop(1, n)
+    def _(d):
+        copy_a(d).start()
+
+    for fill in fills:
+        fill.wait()
+
+    def merge(index, other):
+        rows = part.at[index]
+        step = min(512, width)
+
+        @pl.loop(0, width // step)
+        def _(c):
+            cols = pl.ds(pl.multiple_of(c * step, step), step)
+            rows[:, cols] = (
+                rows[:, cols].astype(jnp.float32) + other[:, cols].astype(jnp.float32)
+            ).astype(part.dtype)
+
+    def one_block(rows, put):
+        gate = jnp.dot(rows, gate_ref[...], preferred_element_type=jnp.float32)
+        up = jnp.dot(rows, up_ref[...], preferred_element_type=jnp.float32)
+        hidden_ref[...] = (gate / (1.0 + jnp.exp(-gate)) * up).astype(hidden_ref.dtype)
+        step = min(512, width)
+
+        @pl.loop(0, width // step)
+        def _(c):
+            cols = pl.ds(pl.multiple_of(c * step, step), step)
+            put(
+                cols,
+                jnp.dot(
+                    hidden_ref[...], down_ref[:, cols], preferred_element_type=jnp.float32
+                ).astype(part.dtype),
+            )
+
+    def compute(j):
+        if slot_count % 16 == 0:
+
+            def put(cols, val):
+                part[j, :, :, cols] = val.reshape(4, slot_count, val.shape[1])
+
+            one_block(slots[j].reshape(4 * slot_count, width), put)
+        else:
+
+            @pl.loop(0, 4)
+            def _(b):
+                def put(cols, val):
+                    part[j, b, :, cols] = val
+
+                one_block(slots[j, b], put)
+
+    def inside(j, low):
+        return jnp.logical_and(j >= low, j < n)
+
+    @pl.loop(0, n + 5)
+    def _(i):
+        @pl.when(inside(i, 1))
+        def _():
+            copy_a(i).wait_recv()
+            copy_y(i).start()
+            copy_c(i).start()
+
+        @pl.when(inside(i - 1, 1))
+        def _():
+            copy_y(i - 1).wait_recv()
+            copy_b(i - 1).start()
+
+        @pl.when(inside(i - 5, 0))
+        def _():
+            copy_q(i - 5).wait_recv()
+            merge((i - 5, own_blk), col_in.at[i - 5])
+
+        @pl.when(inside(i - 3, 0))
+        def _():
+            copy_p(i - 3).wait_recv()
+            for y in range(2):
+                merge((i - 3, col * 2 + y), pair_in.at[i - 3, y])
+
+        @pl.when(inside(i - 2, 1))
+        def _():
+            copy_c(i - 2).wait_recv()
+            copy_b(i - 2).wait_recv()
+
+        @pl.when(inside(i - 2, 0))
+        def _():
+            compute(i - 2)
+
+        @pl.when(inside(i - 5, 1))
+        def _():
+            copy_r(i - 5).start()
+
+        @pl.when(inside(i - 3, 0))
+        def _():
+            copy_q(i - 3).start()
+
+        @pl.when(inside(i - 2, 0))
+        def _():
+            copy_p(i - 2).start()
+
+    def collect(d, rows):
+        mix = mix_ref[d]
+        high = mix.astype(jnp.bfloat16)
+        low = (mix - high.astype(jnp.float32)).astype(jnp.bfloat16)
+        both = jnp.dot(high, rows, preferred_element_type=jnp.float32) + jnp.dot(
+            low, rows, preferred_element_type=jnp.float32
+        )
+        return both
+
+    acc[...] = collect(0, part[0, own_blk])
+
+    @pl.loop(1, n)
+    def _(d):
+        copy_r(d).wait_recv()
+        acc[...] += collect(d, back[d])
+
+    res_ref[...] = acc[...].astype(res_ref.dtype)
+
+    @pl.loop(1, n)
+    def _(d):
+        copy_a(d).wait_send()
+        copy_y(d).wait_send()
+        copy_c(d).wait_send()
+        copy_b(d).wait_send()
+        copy_r(d).wait_send()
+
+    @pl.loop(0, n)
+    def _(d):
+        copy_p(d).wait_send()
+        copy_q(d).wait_send()
+
+
+def run_experts(outgoing, mine, gate_w, up_w, down_w, mix):
+    n, capacity, width = outgoing.shape
+    hidden_units = gate_w.shape[1]
+    tokens = mix.shape[1]
+    rows = 4 * capacity if capacity % 16 == 0 else capacity
+    dtype = outgoing.dtype
+    vmem = pl.BlockSpec(memory_space=pltpu.VMEM)
+    flops = 2 * n * 4 * capacity * width * hidden_units * 3
+    return pl.pallas_call(
+        functools.partial(expert_kernel, n),
+        out_shape=jax.ShapeDtypeStruct((tokens, width), dtype),
+        in_specs=[vmem] * 6,
+        out_specs=vmem,
+        scratch_shapes=[
+            pltpu.VMEM((n, 4, capacity, width), dtype),
+            pltpu.VMEM((n, 4, capacity, width), dtype),
+            pltpu.VMEM((n, 2, capacity, width), dtype),
+            pltpu.VMEM((n, capacity, width), dtype),
+            pltpu.VMEM((n, capacity, width), dtype),
+            pltpu.VMEM((rows, hidden_units), dtype),
+            pltpu.VMEM((tokens, width), jnp.float32),
+        ]
+        + [pltpu.SemaphoreType.DMA((n,))] * 14
+        + [pltpu.SemaphoreType.DMA((4,))],
+        compiler_params=pltpu.CompilerParams(
+            collective_id=0, has_side_effects=True, vmem_limit_bytes=60 * 1024 * 1024
+        ),
+        cost_estimate=pl.CostEstimate(
+            flops=40 * flops, bytes_accessed=16 * 1024 * 1024, transcendentals=0
+        ),
+    )(outgoing, mine, gate_w, up_w, down_w, mix)
+
+
+def expert_part(moe_rows, moe_gain, routes, route_weights, w_gate, w_up, w_down):
+    experts = lax.axis_size("ep")
+    tp_count = lax.axis_size("tp")
+    me = lax.axis_index("ep")
+    tp_id = lax.axis_index("tp")
+    dev_rows = moe_rows.shape[0] // tp_count
+    top_count = routes.shape[1]
+    capacity = max(2, 2 * dev_rows * top_count // experts)
+    width = moe_rows.shape[1]
+    normed = (
+        rms_scaled(moe_rows.astype(jnp.float32), moe_gain)
+        .astype(jnp.bfloat16)
+        .reshape(tp_count, dev_rows, width)
+    )
+    relative = ((routes - me) % experts).reshape(tp_count, dev_rows, top_count)
+    hits = relative[..., None] == lax.iota(jnp.int32, experts)
+    named = jnp.any(hits, axis=2)
+    before = (
+        lax.iota(jnp.int32, dev_rows)[:, None] > lax.iota(jnp.int32, dev_rows)[None, :]
+    ).astype(jnp.bfloat16)
+    places = jnp.einsum(
+        "ij,bjd->bid", before, named.astype(jnp.bfloat16), preferred_element_type=jnp.float32
+    ).astype(jnp.int32)
+    places = jnp.where(named, places, -1)
+    slot_iota = lax.iota(jnp.int32, capacity)
+    take_mine = (places[:, None, :, 0] == slot_iota[None, :, None]).astype(jnp.bfloat16)
+    mine = jnp.einsum(
+        "bst,btm->bsm", take_mine, normed, preferred_element_type=jnp.float32
+    ).astype(jnp.bfloat16)
+    own = lambda arr: lax.dynamic_index_in_dim(arr, tp_id, 0, keepdims=False)
+    own_places = own(places)
+    own_rows = own(normed)
+    take = (own_places.T[:, None, :] == slot_iota[None, :, None]).astype(jnp.bfloat16)
+    outgoing = (
+        jnp.dot(
+            take.reshape(experts * capacity, dev_rows),
+            own_rows,
+            preferred_element_type=jnp.float32,
+        )
+        .astype(jnp.bfloat16)
+        .reshape(experts, capacity, width)
+    )
+    own_weights = own(route_weights.reshape(tp_count, dev_rows, top_count))
+    weight_of = jnp.sum(jnp.where(own(hits), own_weights[..., None], 0.0), axis=1)
+    mix = jnp.where(
+        own_places.T[:, :, None] == slot_iota[None, None, :], weight_of.T[:, :, None], 0.0
+    )
+    return run_experts(outgoing, mine, w_gate[0], w_up[0], w_down[0], mix)
 
 
 def local(
@@ -57,8 +371,10 @@
     start_total = jnp.zeros((positions, kv_heads, per_key, 2), jnp.float32)
     start_acc = jnp.zeros((positions, kv_heads, per_key, 2, value_dim), jnp.float32)
     carry = (start_max, start_total, start_acc)
-    key_piece = lax.all_gather(keys, "ep", axis=0, tiled=True)
-    value_piece = lax.all_gather(values, "ep", axis=0, tiled=True)
+    both = jnp.concatenate([keys, values], axis=2)
+    gathered = lax.all_gather(both, "ep", axis=0, tiled=True)
+    key_piece = gathered[:, :, : keys.shape[2]]
+    value_piece = gathered[:, :, keys.shape[2] :]
     shard_count = key_piece.shape[0] // positions
     together = 1
     for candidate in (2, 3, 4):
@@ -123,43 +439,7 @@
         w_out,
         preferred_element_type=jnp.float32,
     ).astype(jnp.bfloat16)
-    experts = lax.axis_size("ep")
-    dev_rows = moe_rows.shape[0] // tp_count
-    top_count = routes.shape[1]
-    capacity = max(2, 2 * dev_rows * top_count // experts)
-    model_width = moe_rows.shape[1]
-    hidden_units = w_gate.shape[2]
-    own_routes = lax.dynamic_slice_in_dim(routes, tp_id * dev_rows, dev_rows, 0)
-    own_weights = lax.dynamic_slice_in_dim(route_weights, tp_id * dev_rows, dev_rows, 0)
-    own_rows = rms_scaled(
-        lax.dynamic_slice_in_dim(moe_rows, tp_id * dev_rows, dev_rows, 0).astype(jnp.float32),
-        moe_gain,
-    ).astype(jnp.bfloat16)
-    outgoing, own_slots = fill_slots(own_rows, own_routes, experts, capacity)
-    arrived = lax.all_to_all(outgoing, "ep", split_axis=0, concat_axis=0, tiled=True)
-    slot_rows = lax.all_gather(arrived[None], "tp", axis=0, tiled=True)
-    flat_rows = slot_rows.reshape(-1, model_width)
-    gate_out = jnp.dot(flat_rows, w_gate[0], preferred_element_type=jnp.float32)
-    up_out = jnp.dot(flat_rows, w_up[0], preferred_element_type=jnp.float32)
-    hidden = (
-        (jax.nn.silu(gate_out) * up_out)
-        .astype(jnp.bfloat16)
-        .reshape(slot_rows.shape[:-1] + (hidden_units,))
-    )
-    flat_terms = hidden.reshape(-1, hidden_units)
-    summed = lax.psum_scatter(
-        jnp.dot(flat_terms, w_down[0], preferred_element_type=jnp.float32)
-        .reshape(hidden.shape[:-1] + (model_width,))
-        .astype(jnp.bfloat16),
-        "tp",
-        scatter_dimension=0,
-        tiled=True,
-    )
-    returned = lax.all_to_all(summed, "ep", split_axis=1, concat_axis=1, tiled=True)[0]
-    picked = returned[own_routes, own_slots]
-    moe_out = jnp.sum(own_weights[..., None] * picked.astype(jnp.float32), axis=1).astype(
-        jnp.bfloat16
-    )
+    moe_out = expert_part(moe_rows, moe_gain, routes, route_weights, w_gate, w_up, w_down)
     return (mixer_out, moe_out)
 
 

time: 331 us -> 218 us (0.66)
  the two profiles are of different devices: /device:TPU:16 before, /device:TPU:0 now
where the time goes in v1:
time: 218 us
  Pallas kernels  136 us (62%)
  waiting for transfers between devices  34.8 us (16%)
  between operations  14.3 us (7%)
  other arithmetic  11.1 us (5%)
  matrix products  8.78 us (4%)
  local copies, waits for them, and re-layouts  7.47 us (3%)
  starting transfers between devices  3.98 us (2%)
    pallas_call x1, Pallas kernels, run_experts(): pl.pallas_call(functools.partial(expert_kernel, n), out_shape=jax.ShapeDt...  136 us
    all_gather x1, waiting for transfers between devices, local(): gathered = lax.all_gather(both, 'ep', axis=0, tiled=True)  34.8 us
  transfers between devices with their start and end apart: 2, of which 1 were waited for; matrix products, arithmetic and copies ran while one was open for 5% of the time, Pallas kernels for 62%

profile of v1, /device:TPU:0, one launch (start us, length us, event | category | flops | bytes accessed | tf_op | source)
XLA Modules:
  0.0 217.7 jit_solution(12787285143807136239)
XLA Ops:
  7.2 1.7 pad_maximum_fusion
  9.0 0.7 fusion.41
  9.8 2.1 fusion.23
  12.0 1.0 copy.76
  13.1 1.2 fusion.25
  14.4 2.0 convolution_convert_fusion
  16.4 1.1 fusion.30.mix_ref
  17.5 1.4 convolution_convert_fusion.1.mine_ref
  19.0 34.8 %all-gather.2.cloned.1.call-done = bf16[2048,1,256]{2,0,1:T(8,128)(2,1)} async-done(((bf16[256,1,256]{2,0,1:T(8,128)(2,1)}), bf16[2048,1,256]{2,0,1:T(8,128)(2,1)}) %all-gather.2.cloned.1.call-update) | async-done | bytes 1048592 | tf_op jit(solution)/shard_map/all_gather | solution.py:375
  53.7 1.3 fusion.45
  55.0 0.4 reshape.222
  55.4 0.7 copy.77
  56.2 0.2 copy.79
  56.5 6.3 %while.15 = (s32[]{:T(128)}, f32[256,1,2,2]{0,2,3,1:T(2,128)S(1)}, f32[256,1,2,2]{0,2,3,1:T(2,128)S(1)}, f32[256,1,2,2,128]{0,4,3,2,1:T(8,128)S(1)}, s32[2]{0:T(...) while((s32[]{:T(128)}, f32[256,1,2,2]{0,2,3,1:T(2,128)S(1)}, ...), condition=%wide.region_5.6_spmd.clone, body=%wide.region_0.5_spmd.clone.sunk | while | flops 411570432 | bytes 15155495 | solution.py:420
  56.5 0.7 dynamic_slice.61
  57.9 3.5 %conditional.3 = ((f32[256,1,2,2]{0,2,3,1:T(2,128)S(1)}, f32[256,1,2,2]{0,2,3,1:T(2,128)S(1)}, f32[256,1,2,2,128]{0,4,3,2,1:T(8,128)S(1)})) conditional(s32[]{:T(128)} %convert_element_type.70, (f32[256,1,2,2]{0,2,3,1:T(2,128)S(1)}, f32[256,1,2,2]{0,2,3,1:T(2,128)S(1)}, f32[256,1,2,2,128]{0,4,3,2,1:T(8,128)S(1)}) %tuple.50, (s32[]{:T(128)}, ...), branch_computations={%region_1.1_spmd, %region_2.4_spmd} | conditional | flops 411570432 | bytes 15154224 | solution.py:418
  57.9 0.7 iota_add_fusion
  58.6 0.2 broadcast_compare_fusion
  58.8 0.9 fusion.4
  59.7 1.0 fusion.5
  60.8 0.5 fusion.11
  61.4 0.7 dynamic_slice.61
  62.8 0.2 copy.81
  63.0 0.1 copy.80
  63.2 0.7 broadcast_divide_fusion
  63.9 0.4 fusion.33
  64.4 1.0 fusion.37
  65.4 3.9 %all-to-all-start = ((bf16[256,2,128]{2,1,0:T(2,128)(2,1)}), bf16[256,2,128]{2,1,0:T(2,128)(2,1)}, u32[]{:S(2)}, u32[]{:S(2)}) async-start(bf16[256,2,128]{2,1,0:T(2,128)(2,1)} %fusion.37), calls=%async_computation | async-start | bytes 262144 | tf_op jit(solution)/shard_map/all_to_all | solution.py:430
  69.3 135.8 %shard_map.140 = bf16[128,2048]{1,0:T(8,128)(2,1)} custom-call(bf16[8,64,2048]{2,1,0:T(8,128)(2,1)} %bitcast.121, bf16[4,64,2048]{2,1,0:T(8,128)(2,1)} %convolution_convert_fusion.1.mine_ref, bf16[2048,256]{1,0:T(8,128)(2,1)} %bitcast.130, bf16[2048,256]{1,0:T(8,128)(2,1)} %bitcast.131, bf16[256,2048]{1,0:T(8,128)(2,1)} %bitcast.132, ...), custom_call_target="tpu_custom_call" | custom-call | flops 257698037760 | bytes 16777216 | tf_op jit(solution)/shard_map/pallas_call | solution.py:269
  205.1 1.0 copy.84
  206.3 3.7 %convolution_convert_fusion.2 = bf16[64,2048]{1,0:T(8,128)(2,1)} fusion(bf16[64,1024]{1,0:T(8,128)(2,1)S(1)} %reshape.215, bf16[1024,2048]{1,0:T(8,128)(2,1)} %param.22), kind=kOutput, calls=%fused_computation.33 | convolution fusion | flops 268566528 | bytes 4587520 | tf_op jit(solution)/shard_map/dot_general | solution.py:437
  210.1 0.8 copy.123
  (37 shorter events, 0.7 us)
Async XLA Ops:
  7.2 4.8 %copy-start = (f32[512,2]{0,1:T(2,128)S(1)}, f32[512,2]{0,1:T(2,128)}, u32[]{:S(2)}) copy-start(f32[512,2]{0,1:T(2,128)} %param.26) | copy-start | bytes 12292
  7.2 5.9 %copy-start.1 = (bf16[512,2048]{1,0:T(8,128)(2,1)S(1)}, bf16[512,2048]{1,0:T(8,128)(2,1)}, u32[]{:S(2)}) copy-start(bf16[512,2048]{1,0:T(8,128)(2,1)} %param.23) | copy-start | bytes 6291460
  7.2 46.5 %all-gather.2.cloned.1.call-start = ((), (), s32[]{:S(2)}) async-start(), calls=%async_computation.1 | async-start | bytes 1179648 | tf_op jit(solution)/shard_map/all_gather | solution.py:375
  56.5 7.4 %copy-start.3 = (f32[2]{0:T(128)S(1)}, f32[2]{0:T(128)}, u32[]{:S(2)}) copy-start(f32[2]{0:T(128)} %param.20) | copy-start | bytes 28
  56.5 7.9 %copy-start.4 = (f32[128]{0:T(128)S(1)}, f32[128]{0:T(128)}, u32[]{:S(2)}) copy-start(f32[128]{0:T(128)} %param.21) | copy-start | bytes 1540
  65.4 139.7 %all-to-all-start = ((bf16[256,2,128]{2,1,0:T(2,128)(2,1)}), bf16[256,2,128]{2,1,0:T(2,128)(2,1)}, u32[]{:S(2)}, u32[]{:S(2)}) async-start(bf16[256,2,128]{2,1,0:T(2,128)(2,1)} %fusion.37), calls=%async_computation | async-start | bytes 262144 | tf_op jit(solution)/shard_map/all_to_all | solution.py:430
  205.1 5.0 %copy-start.2 = (bf16[128,2048]{1,0:T(8,128)(2,1)S(1)}, bf16[128,2048]{1,0:T(8,128)(2,1)}, u32[]{:S(2)}) copy-start(bf16[128,2048]{1,0:T(8,128)(2,1)} %shard_map.140) | copy-start | bytes 1572868
Sparse Core Ops, SparseCore 0:
  10.7 42.9 all-gather.1

commit v2 on v1

--- a/solution.py
+++ b/solution.py
@@ -19,6 +19,7 @@
 def expert_kernel(
     n,
     out_ref,
+    near_ref,
     mine_ref,
     gate_ref,
     up_ref,
@@ -61,6 +62,15 @@
     slot_count = slots.shape[2]
     width = slots.shape[3]
 
+    near = near_ref.shape[0]
+    bits = [1 << b for b in range(n.bit_length() - 1)]
+
+    def partner(d):
+        total = 0
+        for bit in bits:
+            total = total + (me // bit + d // bit) % 2 * bit
+        return total
+
     def remote(src, dst, ssem, rsem, ep_id, tp_id):
         return pltpu.make_async_remote_copy(
             src_ref=src,
@@ -76,7 +86,7 @@
     @pl.loop(1, n)
     def _(d):
         pl.semaphore_signal(
-            barrier, inc=1, device_id=((me + d) % n, tp), device_id_type=pl.DeviceIdType.MESH
+            barrier, inc=1, device_id=(partner(d), tp), device_id_type=pl.DeviceIdType.MESH
         )
 
     for peer in (pair_peer, row_peer):
@@ -95,7 +105,12 @@
 
     def copy_a(d):
         return remote(
-            out_ref.at[d], slots.at[d, own_blk], send_a.at[d], recv_a.at[d], (me + d) % n, tp
+            out_ref.at[d], slots.at[d, own_blk], send_a.at[d], recv_a.at[d], partner(d), tp
+        )
+
+    def copy_n(d):
+        return remote(
+            near_ref.at[d], slots.at[d, far_blk], send_y.at[d], recv_y.at[d], partner(d), tp
         )
 
     def copy_y(d):
@@ -125,12 +140,16 @@
 
     def copy_r(d):
         return remote(
-            part.at[d, own_blk], back.at[d], send_r.at[d], recv_r.at[d], (me + n - d) % n, tp
+            part.at[d, own_blk], back.at[d], send_r.at[d], recv_r.at[d], partner(d), tp
         )
 
     @pl.loop(1, n)
     def _(d):
         copy_a(d).start()
+
+        @pl.when(d < near)
+        def _():
+            copy_n(d).start()
 
     for fill in fills:
         fill.wait()
@@ -186,8 +205,11 @@
         @pl.when(inside(i, 1))
         def _():
             copy_a(i).wait_recv()
+            copy_c(i).start()
+
+        @pl.when(inside(i, near))
+        def _():
             copy_y(i).start()
-            copy_c(i).start()
 
         @pl.when(inside(i - 1, 1))
         def _():
@@ -258,7 +280,7 @@
         copy_q(d).wait_send()
 
 
-def run_experts(outgoing, mine, gate_w, up_w, down_w, mix):
+def run_experts(outgoing, nearby, mine, gate_w, up_w, down_w, mix):
     n, capacity, width = outgoing.shape
     hidden_units = gate_w.shape[1]
     tokens = mix.shape[1]
@@ -269,7 +291,7 @@
     return pl.pallas_call(
         functools.partial(expert_kernel, n),
         out_shape=jax.ShapeDtypeStruct((tokens, width), dtype),
-        in_specs=[vmem] * 6,
+        in_specs=[vmem] * 7,
         out_specs=vmem,
         scratch_shapes=[
             pltpu.VMEM((n, 4, capacity, width), dtype),
@@ -288,7 +310,7 @@
         cost_estimate=pl.CostEstimate(
             flops=40 * flops, bytes_accessed=16 * 1024 * 1024, transcendentals=0
         ),
-    )(outgoing, mine, gate_w, up_w, down_w, mix)
+    )(outgoing, nearby, mine, gate_w, up_w, down_w, mix)
 
 
 def expert_part(moe_rows, moe_gain, routes, route_weights, w_gate, w_up, w_down):
@@ -305,7 +327,7 @@
         .astype(jnp.bfloat16)
         .reshape(tp_count, dev_rows, width)
     )
-    relative = ((routes - me) % experts).reshape(tp_count, dev_rows, top_count)
+    relative = jnp.bitwise_xor(routes, me).reshape(tp_count, dev_rows, top_count)
     hits = relative[..., None] == lax.iota(jnp.int32, experts)
     named = jnp.any(hits, axis=2)
     before = (
@@ -321,24 +343,29 @@
         "bst,btm->bsm", take_mine, normed, preferred_element_type=jnp.float32
     ).astype(jnp.bfloat16)
     own = lambda arr: lax.dynamic_index_in_dim(arr, tp_id, 0, keepdims=False)
+    other_id = (1 - tp_id // 2) * 2 + tp_id % 2
     own_places = own(places)
-    own_rows = own(normed)
-    take = (own_places.T[:, None, :] == slot_iota[None, :, None]).astype(jnp.bfloat16)
-    outgoing = (
-        jnp.dot(
-            take.reshape(experts * capacity, dev_rows),
-            own_rows,
-            preferred_element_type=jnp.float32,
-        )
-        .astype(jnp.bfloat16)
-        .reshape(experts, capacity, width)
-    )
+
+    def fill(block, first, last):
+        block_places = lax.dynamic_index_in_dim(places, block, 0, keepdims=False)[:, first:last]
+        block_rows = lax.dynamic_index_in_dim(normed, block, 0, keepdims=False)
+        take = (block_places.T[:, None, :] == slot_iota[None, :, None]).astype(jnp.bfloat16)
+        return (
+            jnp.dot(
+                take.reshape(-1, dev_rows), block_rows, preferred_element_type=jnp.float32
+            )
+            .astype(jnp.bfloat16)
+            .reshape(last - first, capacity, width)
+        )
+
+    outgoing = fill(tp_id, 0, experts)
+    nearby = fill(other_id, 0, experts // 2)
     own_weights = own(route_weights.reshape(tp_count, dev_rows, top_count))
     weight_of = jnp.sum(jnp.where(own(hits), own_weights[..., None], 0.0), axis=1)
     mix = jnp.where(
         own_places.T[:, :, None] == slot_iota[None, None, :], weight_of.T[:, :, None], 0.0
     )
-    return run_experts(outgoing, mine, w_gate[0], w_up[0], w_down[0], mix)
+    return run_experts(outgoing, nearby, mine, w_gate[0], w_up[0], w_down[0], mix)
 
 
 def local(
@@ -373,6 +400,8 @@
     carry = (start_max, start_total, start_acc)
     both = jnp.concatenate([keys, values], axis=2)
     gathered = lax.all_gather(both, "ep", axis=0, tiled=True)
+    moe_out = expert_part(moe_rows, moe_gain, routes, route_weights, w_gate, w_up, w_down)
+    gathered, moe_out = lax.optimization_barrier((gathered, moe_out))
     key_piece = gathered[:, :, : keys.shape[2]]
     value_piece = gathered[:, :, keys.shape[2] :]
     shard_count = key_piece.shape[0] // positions
@@ -439,7 +468,6 @@
         w_out,
         preferred_element_type=jnp.float32,
     ).astype(jnp.bfloat16)
-    moe_out = expert_part(moe_rows, moe_gain, routes, route_weights, w_gate, w_up, w_down)
     return (mixer_out, moe_out)
 
 

time: 218 us -> 198 us (0.908)
  the two profiles are of different devices: /device:TPU:0 before, /device:TPU:16 now
where the time goes in v2:
time: 198 us; the launch traced here: 197 us
  Pallas kernels  143 us (72%)
  between operations  14.3 us (7%)
  other arithmetic  12.9 us (7%)
  matrix products  11.6 us (6%)
  local copies, waits for them, and re-layouts  5.45 us (3%)
  waiting for transfers between devices  4.6 us (2%)
  starting transfers between devices  3.36 us (2%)
    pallas_call x1, Pallas kernels, run_experts(): pl.pallas_call(functools.partial(expert_kernel, n), out_shape=jax.ShapeDt...  143 us
    all_to_all x1, waiting for transfers between devices, local(): lax.all_to_all(attn_rows.reshape(positions, q_heads, value_dim), 'tp', sp...  4.57 us
  transfers between devices with their start and end apart: 2, of which 1 were waited for; matrix products, arithmetic and copies ran while one was open for 5% of the time, Pallas kernels for 73%

profile of v2, /device:TPU:16, one launch (start us, length us, event | category | flops | bytes accessed | tf_op | source)
XLA Modules:
  0.0 197.2 jit_solution(13513505030814962014)
XLA Ops:
  7.2 1.7 pad_maximum_fusion
  9.0 0.7 xor_bitcast_fusion
  9.9 2.1 %fusion.23 = f32[512]{0:T(512)S(1)} fusion(bf16[512,2048]{1,0:T(8,128)(2,1)} %param.23), kind=kLoop, calls=%fused_computation.28 | loop fusion | flops 3145216 | bytes 2099200 | tf_op jit(solution)/shard_map/reduce_sum | solution.py:15
  12.0 1.2 fusion.25
  13.3 2.0 %convolution_convert_fusion = bf16[512,2048]{1,0:T(8,128)(2,1)} fusion(pred[512,128]{1,0:T(32,128)(4,1)S(1)} %bitcast.138, bf16[4,128,2048]{2,1,0:T(8,128)(2,1)S(1)} %bitcast.129, s32[]{:T(128)S(6)} %select_n.45), kind=kOutput, calls=%fused_computation.31 | convolution fusion | flops 269484032 | bytes 2686980 | tf_op jit(solution)/shard_map/dot_general | solution.py:354
  15.3 1.4 convolution_convert_fusion.2
  16.7 1.1 fusion.32.mix_ref
  17.9 1.4 convolution_convert_fusion.1.mine_ref
  19.3 143.4 %shard_map.140 = bf16[128,2048]{1,0:T(8,128)(2,1)} custom-call(bf16[8,64,2048]{2,1,0:T(8,128)(2,1)} %bitcast.132, bf16[4,64,2048]{2,1,0:T(8,128)(2,1)} %bitcast.135, bf16[4,64,2048]{2,1,0:T(8,128)(2,1)} %convolution_convert_fusion.1.mine_ref, bf16[2048,256]{1,0:T(8,128)(2,1)} %bitcast.143, bf16[2048,256]{1,0:T(8,128)(2,1)} %bitcast.144, ...), custom_call_target="tpu_custom_call" | custom-call | flops 257698037760 | bytes 16777216 | tf_op jit(solution)/shard_map/pallas_call | solution.py:291
  162.9 1.3 fusion.47
  164.2 0.4 reshape.260
  164.6 0.7 copy.79
  165.7 9.4 %while.15 = (s32[]{:T(128)}, f32[256,1,2,2]{0,2,3,1:T(2,128)S(1)}, f32[256,1,2,2]{0,2,3,1:T(2,128)S(1)}, f32[256,1,2,2,128]{0,4,3,2,1:T(8,128)S(1)}, s32[2]{0:T(...) while((s32[]{:T(128)}, f32[256,1,2,2]{0,2,3,1:T(2,128)S(1)}, ...), condition=%wide.region_8.9_spmd.clone, body=%wide.region_3.8_spmd.clone.sunk | while | flops 411570432 | bytes 15155487 | solution.py:449
  165.7 0.6 dynamic_slice.77
  166.9 3.4 %conditional.3 = ((f32[256,1,2,2]{0,2,3,1:T(2,128)S(1)}, f32[256,1,2,2]{0,2,3,1:T(2,128)S(1)}, f32[256,1,2,2,128]{0,4,3,2,1:T(8,128)S(1)})) conditional(s32[]{:T(128)} %convert_element_type.76, (f32[256,1,2,2]{0,2,3,1:T(2,128)S(1)}, f32[256,1,2,2]{0,2,3,1:T(2,128)S(1)}, f32[256,1,2,2,128]{0,4,3,2,1:T(8,128)S(1)}) %tuple.53, (s32[]{:T(128)}, ...), branch_computations={%region_4.4_spmd, %region_5.7_spmd} | conditional | flops 411570432 | bytes 15154224 | solution.py:447
  167.0 0.7 iota_add_fusion
  167.9 0.9 fusion.4
  168.7 1.0 fusion.5
  169.8 0.5 fusion.11
  170.4 0.6 dynamic_slice.77
  171.6 3.4 %conditional.3 = ((f32[256,1,2,2]{0,2,3,1:T(2,128)S(1)}, f32[256,1,2,2]{0,2,3,1:T(2,128)S(1)}, f32[256,1,2,2,128]{0,4,3,2,1:T(8,128)S(1)})) conditional(s32[]{:T(128)} %convert_element_type.76, (f32[256,1,2,2]{0,2,3,1:T(2,128)S(1)}, f32[256,1,2,2]{0,2,3,1:T(2,128)S(1)}, f32[256,1,2,2,128]{0,4,3,2,1:T(8,128)S(1)}) %tuple.53, (s32[]{:T(128)}, ...), branch_computations={%region_4.4_spmd, %region_5.7_spmd} | conditional | flops 411570432 | bytes 15154224 | solution.py:447
  171.6 0.7 iota_add_fusion
  172.5 0.9 fusion.4
  173.4 1.0 fusion.5
  174.5 0.5 fusion.11
  175.5 0.7 broadcast_divide_fusion
  176.2 0.4 fusion.35
  176.7 1.0 fusion.39
  177.7 3.3 %all-to-all-start = ((bf16[256,2,128]{2,1,0:T(2,128)(2,1)}), bf16[256,2,128]{2,1,0:T(2,128)(2,1)S(1)}, u32[]{:S(2)}, u32[]{:S(2)}) async-start(bf16[256,2,128]{2,1,0:T(2,128)(2,1)} %fusion.39), calls=%async_computation | async-start | bytes 262144 | tf_op jit(solution)/shard_map/all_to_all | solution.py:459
  181.0 4.6 %all-to-all-done = bf16[256,2,128]{2,1,0:T(2,128)(2,1)S(1)} async-done(((bf16[256,2,128]{2,1,0:T(2,128)(2,1)}), bf16[256,2,128]{2,1,0:T(2,128)(2,1)S(1)}, u32[]{:S(2)}, u32[]{:S(2)}) %all-to-all-start) | async-done | bytes 131104 | tf_op jit(solution)/shard_map/all_to_all | solution.py:459
  185.8 3.7 %convolution_convert_fusion.3 = bf16[64,2048]{1,0:T(8,128)(2,1)} fusion(bf16[64,1024]{1,0:T(8,128)(2,1)S(1)} %reshape.256, bf16[1024,2048]{1,0:T(8,128)(2,1)} %param.22), kind=kOutput, calls=%fused_computation.34 | convolution fusion | flops 268566528 | bytes 4587520 | tf_op jit(solution)/shard_map/dot_general | solution.py:466
  189.6 0.8 copy.126
  (52 shorter events, 1.9 us)
Async XLA Ops:
  7.2 9.6 %copy-start = (f32[512,2]{0,1:T(2,128)S(1)}, f32[512,2]{0,1:T(2,128)}, u32[]{:S(2)}) copy-start(f32[512,2]{0,1:T(2,128)} %param.26) | copy-start | bytes 12292
  7.2 4.8 %copy-start.1 = (bf16[512,2048]{1,0:T(8,128)(2,1)S(1)}, bf16[512,2048]{1,0:T(8,128)(2,1)}, u32[]{:S(2)}) copy-start(bf16[512,2048]{1,0:T(8,128)(2,1)} %param.23) | copy-start | bytes 6291460
  7.2 155.7 %all-gather.2.cloned.1.call-start = ((), (), s32[]{:S(2)}) async-start(), calls=%async_computation.1 | async-start | bytes 1179648 | tf_op jit(solution)/shard_map/all_gather | solution.py:402
  19.3 143.5 %copy-start.3 = (bf16[256,2,128]{2,1,0:T(2,128)(2,1)S(1)}, bf16[256,2,128]{2,1,0:T(2,128)(2,1)}, u32[]{:S(2)}) copy-start(bf16[256,2,128]{2,1,0:T(2,128)(2,1)} %param.17) | copy-start | bytes 393220
  165.7 10.5 %copy-start.4 = (f32[2]{0:T(128)S(1)}, f32[2]{0:T(128)}, u32[]{:S(2)}) copy-start(f32[2]{0:T(128)} %param.20) | copy-start | bytes 28
  165.7 11.0 %copy-start.5 = (f32[128]{0:T(128)S(1)}, f32[128]{0:T(128)}, u32[]{:S(2)}) copy-start(f32[128]{0:T(128)} %param.21) | copy-start | bytes 1540
  175.5 14.1 %copy-start.2 = (bf16[128,2048]{1,0:T(8,128)(2,1)S(1)}, bf16[128,2048]{1,0:T(8,128)(2,1)}, u32[]{:S(2)}) copy-start(bf16[128,2048]{1,0:T(8,128)(2,1)} %shard_map.140) | copy-start | bytes 1572868
  177.7 7.9 %all-to-all-start = ((bf16[256,2,128]{2,1,0:T(2,128)(2,1)}), bf16[256,2,128]{2,1,0:T(2,128)(2,1)S(1)}, u32[]{:S(2)}, u32[]{:S(2)}) async-start(bf16[256,2,128]{2,1,0:T(2,128)(2,1)} %fusion.39), calls=%async_computation | async-start | bytes 262144 | tf_op jit(solution)/shard_map/all_to_all | solution.py:459
Sparse Core Ops, SparseCore 0:
  10.7 64.4 all-gather.1

commit v3 on v2

--- a/solution.py
+++ b/solution.py
@@ -20,6 +20,8 @@
     n,
     out_ref,
     near_ref,
+    rows_ref,
+    take_ref,
     mine_ref,
     gate_ref,
     up_ref,
@@ -31,8 +33,13 @@
     pair_in,
     col_in,
     back,
+    far_rows,
+    far_take,
+    picked,
     hidden_ref,
     acc,
+    send_s,
+    recv_s,
     send_a,
     recv_a,
     send_y,
@@ -63,6 +70,8 @@
     width = slots.shape[3]
 
     near = near_ref.shape[0]
+    half = out_ref.shape[0]
+    bubble = 3
     bits = [1 << b for b in range(n.bit_length() - 1)]
 
     def partner(d):
@@ -108,6 +117,22 @@
             out_ref.at[d], slots.at[d, own_blk], send_a.at[d], recv_a.at[d], partner(d), tp
         )
 
+    def copy_s():
+        return [
+            remote(src, dst, send_s.at[k], recv_s.at[k], partner(half), tp)
+            for k, (src, dst) in enumerate(((take_ref, far_take), (rows_ref, far_rows)))
+        ]
+
+    def copy_g(d):
+        return remote(
+            picked.at[d - half],
+            slots.at[d, own_blk],
+            send_a.at[d],
+            recv_a.at[d],
+            partner(d - half),
+            tp,
+        )
+
     def copy_n(d):
         return remote(
             near_ref.at[d], slots.at[d, far_blk], send_y.at[d], recv_y.at[d], partner(d), tp
@@ -143,7 +168,10 @@
             part.at[d, own_blk], back.at[d], send_r.at[d], recv_r.at[d], partner(d), tp
         )
 
-    @pl.loop(1, n)
+    for swap in copy_s():
+        swap.start()
+
+    @pl.loop(1, half)
     def _(d):
         copy_a(d).start()
 
@@ -197,56 +225,84 @@
 
                 one_block(slots[j, b], put)
 
-    def inside(j, low):
-        return jnp.logical_and(j >= low, j < n)
-
-    @pl.loop(0, n + 5)
+    def pick():
+        for swap in copy_s():
+            swap.wait_recv()
+        step = min(512, width)
+
+        @pl.loop(0, width // step)
+        def _(c):
+            cols = pl.ds(pl.multiple_of(c * step, step), step)
+            rows = jnp.dot(
+                far_take[...], far_rows[:, cols], preferred_element_type=jnp.float32
+            )
+            rows = rows.reshape(half, slot_count, step).astype(picked.dtype)
+            picked[:, :, cols] = rows
+            slots[half, own_blk, :, cols] = rows[0]
+
+        @pl.loop(half + 1, n)
+        def _(d):
+            copy_g(d).start()
+
+    def at_stage(k, low, action):
+        j = k - bubble * (k // (half + bubble))
+
+        @pl.when(
+            jnp.logical_or(
+                jnp.logical_and(k >= low, k < half),
+                jnp.logical_and(k >= max(low, half) + bubble, k < n + bubble),
+            )
+        )
+        def _():
+            action(j)
+
+    def arrive(j):
+        @pl.when(j < half)
+        def _():
+            copy_a(j).wait_recv()
+
+        @pl.when(j == half)
+        def _():
+            pick()
+
+        @pl.when(j > half)
+        def _():
+            copy_g(j).wait_recv()
+
+        copy_c(j).start()
+
+        @pl.when(j >= near)
+        def _():
+            copy_y(j).start()
+
+    def cross(j):
+        copy_y(j).wait_recv()
+        copy_b(j).start()
+
+    def finish(j):
+        copy_q(j).wait_recv()
+        merge((j, own_blk), col_in.at[j])
+
+    def join(j):
+        copy_p(j).wait_recv()
+        for y in range(2):
+            merge((j, col * 2 + y), pair_in.at[j, y])
+
+    def ready(j):
+        copy_c(j).wait_recv()
+        copy_b(j).wait_recv()
+
+    @pl.loop(0, n + 5 + bubble)
     def _(i):
-        @pl.when(inside(i, 1))
-        def _():
-            copy_a(i).wait_recv()
-            copy_c(i).start()
-
-        @pl.when(inside(i, near))
-        def _():
-            copy_y(i).start()
-
-        @pl.when(inside(i - 1, 1))
-        def _():
-            copy_y(i - 1).wait_recv()
-            copy_b(i - 1).start()
-
-        @pl.when(inside(i - 5, 0))
-        def _():
-            copy_q(i - 5).wait_recv()
-            merge((i - 5, own_blk), col_in.at[i - 5])
-
-        @pl.when(inside(i - 3, 0))
-        def _():
-            copy_p(i - 3).wait_recv()
-            for y in range(2):
-                merge((i - 3, col * 2 + y), pair_in.at[i - 3, y])
-
-        @pl.when(inside(i - 2, 1))
-        def _():
-            copy_c(i - 2).wait_recv()
-            copy_b(i - 2).wait_recv()
-
-        @pl.when(inside(i - 2, 0))
-        def _():
-            compute(i - 2)
-
-        @pl.when(inside(i - 5, 1))
-        def _():
-            copy_r(i - 5).start()
-
-        @pl.when(inside(i - 3, 0))
-        def _():
-            copy_q(i - 3).start()
-
-        @pl.when(inside(i - 2, 0))
-        def _():
-            copy_p(i - 2).start()
+        at_stage(i, 1, arrive)
+        at_stage(i - 1, 1, cross)
+        at_stage(i - 5, 0, finish)
+        at_stage(i - 3, 0, join)
+        at_stage(i - 2, 1, ready)
+        at_stage(i - 2, 0, compute)
+        at_stage(i - 5, 1, lambda j: copy_r(j).start())
+        at_stage(i - 3, 0, lambda j: copy_q(j).start())
+        at_stage(i - 2, 0, lambda j: copy_p(j).start())
 
     def collect(d, rows):
         mix = mix_ref[d]
@@ -266,9 +322,19 @@
 
     res_ref[...] = acc[...].astype(res_ref.dtype)
 
+    for swap in copy_s():
+        swap.wait_send()
+
+    @pl.loop(1, half)
+    def _(d):
+        copy_a(d).wait_send()
+
+    @pl.loop(half + 1, n)
+    def _(d):
+        copy_g(d).wait_send()
+
     @pl.loop(1, n)
     def _(d):
-        copy_a(d).wait_send()
         copy_y(d).wait_send()
         copy_c(d).wait_send()
         copy_b(d).wait_send()
@@ -280,8 +346,8 @@
         copy_q(d).wait_send()
 
 
-def run_experts(outgoing, nearby, mine, gate_w, up_w, down_w, mix):
-    n, capacity, width = outgoing.shape
+def run_experts(n, outgoing, nearby, own_rows, far_take, mine, gate_w, up_w, down_w, mix):
+    half, capacity, width = outgoing.shape
     hidden_units = gate_w.shape[1]
     tokens = mix.shape[1]
     rows = 4 * capacity if capacity % 16 == 0 else capacity
@@ -291,7 +357,7 @@
     return pl.pallas_call(
         functools.partial(expert_kernel, n),
         out_shape=jax.ShapeDtypeStruct((tokens, width), dtype),
-        in_specs=[vmem] * 7,
+        in_specs=[vmem] * 9,
         out_specs=vmem,
         scratch_shapes=[
             pltpu.VMEM((n, 4, capacity, width), dtype),
@@ -299,9 +365,13 @@
             pltpu.VMEM((n, 2, capacity, width), dtype),
             pltpu.VMEM((n, capacity, width), dtype),
             pltpu.VMEM((n, capacity, width), dtype),
+            pltpu.VMEM(own_rows.shape, dtype),
+            pltpu.VMEM(far_take.shape, dtype),
+            pltpu.VMEM((half, capacity, width), dtype),
             pltpu.VMEM((rows, hidden_units), dtype),
             pltpu.VMEM((tokens, width), jnp.float32),
         ]
+        + [pltpu.SemaphoreType.DMA((2,))] * 2
         + [pltpu.SemaphoreType.DMA((n,))] * 14
         + [pltpu.SemaphoreType.DMA((4,))],
         compiler_params=pltpu.CompilerParams(
@@ -310,7 +380,7 @@
         cost_estimate=pl.CostEstimate(
             flops=40 * flops, bytes_accessed=16 * 1024 * 1024, transcendentals=0
         ),
-    )(outgoing, nearby, mine, gate_w, up_w, down_w, mix)
+    )(outgoing, nearby, own_rows, far_take, mine, gate_w, up_w, down_w, mix)
 
 
 def expert_part(moe_rows, moe_gain, routes, route_weights, w_gate, w_up, w_down):
@@ -346,26 +416,33 @@
     other_id = (1 - tp_id // 2) * 2 + tp_id % 2
     own_places = own(places)
 
-    def fill(block, first, last):
-        block_places = lax.dynamic_index_in_dim(places, block, 0, keepdims=False)[:, first:last]
-        block_rows = lax.dynamic_index_in_dim(normed, block, 0, keepdims=False)
-        take = (block_places.T[:, None, :] == slot_iota[None, :, None]).astype(jnp.bfloat16)
-        return (
-            jnp.dot(
-                take.reshape(-1, dev_rows), block_rows, preferred_element_type=jnp.float32
-            )
-            .astype(jnp.bfloat16)
-            .reshape(last - first, capacity, width)
-        )
-
-    outgoing = fill(tp_id, 0, experts)
-    nearby = fill(other_id, 0, experts // 2)
+    half = experts // 2
+
+    def takes(block_places):
+        hits = block_places.T[:, None, :] == slot_iota[None, :, None]
+        return hits.astype(jnp.bfloat16).reshape(-1, dev_rows)
+
+    def fill(take, block_rows):
+        filled = jnp.dot(take, block_rows, preferred_element_type=jnp.float32)
+        return filled.astype(jnp.bfloat16).reshape(-1, capacity, width)
+
+    own_rows = own(normed)
+    own_take = takes(own_places)
+    outgoing = fill(own_take[: half * capacity], own_rows)
+    far_take = own_take[half * capacity :]
+    near = max(2, half - 1)
+    nearby = fill(
+        takes(lax.dynamic_index_in_dim(places, other_id, 0, keepdims=False)[:, :near]),
+        lax.dynamic_index_in_dim(normed, other_id, 0, keepdims=False),
+    )
     own_weights = own(route_weights.reshape(tp_count, dev_rows, top_count))
     weight_of = jnp.sum(jnp.where(own(hits), own_weights[..., None], 0.0), axis=1)
     mix = jnp.where(
         own_places.T[:, :, None] == slot_iota[None, None, :], weight_of.T[:, :, None], 0.0
     )
-    return run_experts(outgoing, nearby, mine, w_gate[0], w_up[0], w_down[0], mix)
+    return run_experts(
+        experts, outgoing, nearby, own_rows, far_take, mine, w_gate[0], w_up[0], w_down[0], mix
+    )
 
 
 def local(

time: 198 us -> 211 us (1.066)
  Pallas kernels: 143 us -> 157 us
    pallas_call x1, Pallas kernels: 143 us -> 157 us  [run_experts(): pl.pallas_call(functools.partial(expert_kernel, n), out_shape=jax.ShapeDt...]
  transfers between devices with their start and end apart: 2 -> 2, of which waited for: 1 -> 1; matrix products, arithmetic and copies ran while one was open for 5% -> 5% of each run, Pallas kernels for 73% -> 74%
where the time goes in v3:
time: 211 us
  Pallas kernels  157 us (74%)
  between operations  14.3 us (7%)
  other arithmetic  13.6 us (6%)
  matrix products  10.8 us (5%)
  local copies, waits for them, and re-layouts  5.5 us (3%)
  waiting for transfers between devices  4.6 us (2%)
  starting transfers between devices  3.36 us (2%)
    pallas_call x1, Pallas kernels, run_experts(): pl.pallas_call(functools.partial(expert_kernel, n), out_shape=jax.ShapeDt...  157 us
    all_to_all x1, waiting for transfers between devices, local(): lax.all_to_all(attn_rows.reshape(positions, q_heads, value_dim), 'tp', sp...  4.57 us
  transfers between devices with their start and end apart: 2, of which 1 were waited for; matrix products, arithmetic and copies ran while one was open for 5% of the time, Pallas kernels for 74%

profile of v3, /device:TPU:16, one launch (start us, length us, event | category | flops | bytes accessed | tf_op | source)
XLA Modules:
  0.0 210.5 jit_solution(16149991741538828066)
XLA Ops:
  7.2 1.7 pad_maximum_fusion
  9.0 0.7 xor_bitcast_fusion
  9.9 0.6 slice_convert_fusion
  10.5 2.1 fusion.23
  12.6 1.2 fusion.25
  14.0 1.2 convolution_convert_fusion.2
  15.2 1.1 fusion.30.mix_ref
  16.4 1.4 convolution_convert_fusion.mine_ref
  17.8 1.4 convolution_convert_fusion.1
  19.2 156.8 %shard_map.140 = bf16[128,2048]{1,0:T(8,128)(2,1)} custom-call(bf16[4,64,2048]{2,1,0:T(8,128)(2,1)} %bitcast.135, bf16[3,64,2048]{2,1,0:T(8,128)(2,1)} %bitcast.136, bf16[128,2048]{1,0:T(8,128)(2,1)} %copy-done.2, bf16[256,128]{1,0:T(8,128)(2,1)} %bitcast.142, bf16[4,64,2048]{2,1,0:T(8,128)(2,1)} %convolution_convert_fusion.mine_ref, ...), custom_call_target="tpu_custom_call" | custom-call | flops 257698037760 | bytes 16777216 | tf_op jit(solution)/shard_map/pallas_call | solution.py:357
  176.2 1.3 fusion.44
  177.9 0.7 copy.79
  179.0 9.4 %while.15 = (s32[]{:T(128)}, f32[256,1,2,2]{0,2,3,1:T(2,128)S(1)}, f32[256,1,2,2]{0,2,3,1:T(2,128)S(1)}, f32[256,1,2,2,128]{0,4,3,2,1:T(8,128)S(1)}, s32[2]{0:T(...) while((s32[]{:T(128)}, f32[256,1,2,2]{0,2,3,1:T(2,128)S(1)}, ...), condition=%wide.region_8.9_spmd.clone, body=%wide.region_3.8_spmd.clone.sunk | while | flops 411570432 | bytes 15155487 | solution.py:526
  179.0 0.6 dynamic_slice.73
  180.3 3.4 %conditional.3 = ((f32[256,1,2,2]{0,2,3,1:T(2,128)S(1)}, f32[256,1,2,2]{0,2,3,1:T(2,128)S(1)}, f32[256,1,2,2,128]{0,4,3,2,1:T(8,128)S(1)})) conditional(s32[]{:T(128)} %convert_element_type.76, (f32[256,1,2,2]{0,2,3,1:T(2,128)S(1)}, f32[256,1,2,2]{0,2,3,1:T(2,128)S(1)}, f32[256,1,2,2,128]{0,4,3,2,1:T(8,128)S(1)}) %tuple.54, (s32[]{:T(128)}, ...), branch_computations={%region_4.4_spmd, %region_5.7_spmd} | conditional | flops 411570432 | bytes 15154224 | solution.py:524
  180.3 0.7 iota_add_fusion
  181.2 0.9 fusion.4
  182.1 1.0 fusion.5
  183.1 0.5 fusion.11
  183.7 0.6 dynamic_slice.73
  184.9 3.4 %conditional.3 = ((f32[256,1,2,2]{0,2,3,1:T(2,128)S(1)}, f32[256,1,2,2]{0,2,3,1:T(2,128)S(1)}, f32[256,1,2,2,128]{0,4,3,2,1:T(8,128)S(1)})) conditional(s32[]{:T(128)} %convert_element_type.76, (f32[256,1,2,2]{0,2,3,1:T(2,128)S(1)}, f32[256,1,2,2]{0,2,3,1:T(2,128)S(1)}, f32[256,1,2,2,128]{0,4,3,2,1:T(8,128)S(1)}) %tuple.54, (s32[]{:T(128)}, ...), branch_computations={%region_4.4_spmd, %region_5.7_spmd} | conditional | flops 411570432 | bytes 15154224 | solution.py:524
  185.0 0.7 iota_add_fusion
  185.8 0.9 fusion.4
  186.7 1.0 fusion.5
  187.8 0.5 fusion.11
  188.8 0.7 broadcast_divide_fusion
  189.5 0.4 fusion.33
  190.0 1.0 fusion.37
  191.0 3.3 %all-to-all-start = ((bf16[256,2,128]{2,1,0:T(2,128)(2,1)}), bf16[256,2,128]{2,1,0:T(2,128)(2,1)S(1)}, u32[]{:S(2)}, u32[]{:S(2)}) async-start(bf16[256,2,128]{2,1,0:T(2,128)(2,1)} %fusion.37), calls=%async_computation | async-start | bytes 262144 | tf_op jit(solution)/shard_map/all_to_all | solution.py:536
  194.3 4.6 %all-to-all-done = bf16[256,2,128]{2,1,0:T(2,128)(2,1)S(1)} async-done(((bf16[256,2,128]{2,1,0:T(2,128)(2,1)}), bf16[256,2,128]{2,1,0:T(2,128)(2,1)S(1)}, u32[]{:S(2)}, u32[]{:S(2)}) %all-to-all-start) | async-done | bytes 131104 | tf_op jit(solution)/shard_map/all_to_all | solution.py:536
  199.1 3.7 %convolution_convert_fusion.3 = bf16[64,2048]{1,0:T(8,128)(2,1)} fusion(bf16[64,1024]{1,0:T(8,128)(2,1)S(1)} %reshape.227, bf16[1024,2048]{1,0:T(8,128)(2,1)} %param.22), kind=kOutput, calls=%fused_computation.34 | convolution fusion | flops 268566528 | bytes 4587520 | tf_op jit(solution)/shard_map/dot_general | solution.py:543
  202.9 0.8 copy.127
  (56 shorter events, 2.3 us)
Async XLA Ops:
  7.2 8.0 %copy-start = (f32[512,2]{0,1:T(2,128)S(1)}, f32[512,2]{0,1:T(2,128)}, u32[]{:S(2)}) copy-start(f32[512,2]{0,1:T(2,128)} %param.26) | copy-start | bytes 12292
  7.2 5.4 %copy-start.1 = (bf16[512,2048]{1,0:T(8,128)(2,1)S(1)}, bf16[512,2048]{1,0:T(8,128)(2,1)}, u32[]{:S(2)}) copy-start(bf16[512,2048]{1,0:T(8,128)(2,1)} %param.23) | copy-start | bytes 6291460
  7.2 169.0 %all-gather.2.cloned.1.call-start = ((), (), s32[]{:S(2)}) async-start(), calls=%async_computation.1 | async-start | bytes 1179648 | tf_op jit(solution)/shard_map/all_gather | solution.py:479
  13.9 5.3 %copy-start.2 = (bf16[128,2048]{1,0:T(8,128)(2,1)}, bf16[128,2048]{1,0:T(8,128)(2,1)S(1)}, u32[]{:S(2)}) copy-start(bf16[128,2048]{1,0:T(8,128)(2,1)S(1)} %dynamic-slice_bitcast_fusion.rows_ref) | copy-start | bytes 1572868
  19.2 156.8 %copy-start.4 = (bf16[256,2,128]{2,1,0:T(2,128)(2,1)S(1)}, bf16[256,2,128]{2,1,0:T(2,128)(2,1)}, u32[]{:S(2)}) copy-start(bf16[256,2,128]{2,1,0:T(2,128)(2,1)} %param.17) | copy-start | bytes 393220
  179.0 10.5 %copy-start.5 = (f32[2]{0:T(128)S(1)}, f32[2]{0:T(128)}, u32[]{:S(2)}) copy-start(f32[2]{0:T(128)} %param.20) | copy-start | bytes 28
  179.0 11.0 %copy-start.6 = (f32[128]{0:T(128)S(1)}, f32[128]{0:T(128)}, u32[]{:S(2)}) copy-start(f32[128]{0:T(128)} %param.21) | copy-start | bytes 1540
  188.8 14.1 %copy-start.3 = (bf16[128,2048]{1,0:T(8,128)(2,1)S(1)}, bf16[128,2048]{1,0:T(8,128)(2,1)}, u32[]{:S(2)}) copy-start(bf16[128,2048]{1,0:T(8,128)(2,1)} %shard_map.140) | copy-start | bytes 1572868
  191.0 7.9 %all-to-all-start = ((bf16[256,2,128]{2,1,0:T(2,128)(2,1)}), bf16[256,2,128]{2,1,0:T(2,128)(2,1)S(1)}, u32[]{:S(2)}, u32[]{:S(2)}) async-start(bf16[256,2,128]{2,1,0:T(2,128)(2,1)} %fusion.37), calls=%async_computation | async-start | bytes 262144 | tf_op jit(solution)/shard_map/all_to_all | solution.py:536
Sparse Core Ops, SparseCore 0:
  10.7 56.6 all-gather.1

commit v4 on v2

--- a/solution.py
+++ b/solution.py
@@ -21,11 +21,13 @@
     out_ref,
     near_ref,
     mine_ref,
+    kv_ref,
     gate_ref,
     up_ref,
     down_ref,
     mix_ref,
     res_ref,
+    kv_out,
     slots,
     part,
     pair_in,
@@ -33,6 +35,8 @@
     back,
     hidden_ref,
     acc,
+    send_k,
+    recv_k,
     send_a,
     recv_a,
     send_y,
@@ -93,6 +97,8 @@
         pl.semaphore_signal(
             barrier, inc=1, device_id=(me, peer), device_id_type=pl.DeviceIdType.MESH
         )
+    keep = pltpu.make_async_copy(kv_ref, kv_out.at[me], local_sem.at[4])
+    keep.start()
     fills = [
         pltpu.make_async_copy(
             mine_ref.at[b], slots.at[0, (b % 2) * 2 + b // 2], local_sem.at[b]
@@ -107,6 +113,13 @@
         return remote(
             out_ref.at[d], slots.at[d, own_blk], send_a.at[d], recv_a.at[d], partner(d), tp
         )
+
+    def copy_k(d):
+        return remote(kv_ref, kv_out.at[me], send_k.at[d], recv_k.at[d], partner(d), tp)
+
+    def copy_f(d):
+        block = kv_out.at[partner(near)]
+        return remote(block, block, send_k.at[d], recv_k.at[d], partner(d - near), tp)
 
     def copy_n(d):
         return remote(
@@ -150,6 +163,12 @@
         @pl.when(d < near)
         def _():
             copy_n(d).start()
+
+    copy_k(near).start()
+
+    @pl.loop(1, near)
+    def _(d):
+        copy_k(d).start()
 
     for fill in fills:
         fill.wait()
@@ -211,6 +230,14 @@
         def _():
             copy_y(i).start()
 
+        @pl.when(i == near)
+        def _():
+            copy_k(near).wait_recv()
+
+            @pl.loop(near + 1, n)
+            def _(d):
+                copy_f(d).start()
+
         @pl.when(inside(i - 1, 1))
         def _():
             copy_y(i - 1).wait_recv()
@@ -264,6 +291,17 @@
         copy_r(d).wait_recv()
         acc[...] += collect(d, back[d])
 
+    @pl.loop(1, near)
+    def _(d):
+        copy_k(d).wait()
+
+    copy_k(near).wait_send()
+
+    @pl.loop(near + 1, n)
+    def _(d):
+        copy_f(d).wait()
+
+    keep.wait()
     res_ref[...] = acc[...].astype(res_ref.dtype)
 
     @pl.loop(1, n)
@@ -280,7 +318,7 @@
         copy_q(d).wait_send()
 
 
-def run_experts(outgoing, nearby, mine, gate_w, up_w, down_w, mix):
+def run_experts(outgoing, nearby, mine, kv, gate_w, up_w, down_w, mix):
     n, capacity, width = outgoing.shape
     hidden_units = gate_w.shape[1]
     tokens = mix.shape[1]
@@ -290,9 +328,12 @@
     flops = 2 * n * 4 * capacity * width * hidden_units * 3
     return pl.pallas_call(
         functools.partial(expert_kernel, n),
-        out_shape=jax.ShapeDtypeStruct((tokens, width), dtype),
-        in_specs=[vmem] * 7,
-        out_specs=vmem,
+        out_shape=(
+            jax.ShapeDtypeStruct((tokens, width), dtype),
+            jax.ShapeDtypeStruct((n,) + kv.shape, kv.dtype),
+        ),
+        in_specs=[vmem] * 8,
+        out_specs=(vmem, pl.BlockSpec(memory_space=pl.ANY)),
         scratch_shapes=[
             pltpu.VMEM((n, 4, capacity, width), dtype),
             pltpu.VMEM((n, 4, capacity, width), dtype),
@@ -302,18 +343,18 @@
             pltpu.VMEM((rows, hidden_units), dtype),
             pltpu.VMEM((tokens, width), jnp.float32),
         ]
-        + [pltpu.SemaphoreType.DMA((n,))] * 14
-        + [pltpu.SemaphoreType.DMA((4,))],
+        + [pltpu.SemaphoreType.DMA((n,))] * 16
+        + [pltpu.SemaphoreType.DMA((5,))],
         compiler_params=pltpu.CompilerParams(
             collective_id=0, has_side_effects=True, vmem_limit_bytes=60 * 1024 * 1024
         ),
         cost_estimate=pl.CostEstimate(
             flops=40 * flops, bytes_accessed=16 * 1024 * 1024, transcendentals=0
         ),
-    )(outgoing, nearby, mine, gate_w, up_w, down_w, mix)
-
-
-def expert_part(moe_rows, moe_gain, routes, route_weights, w_gate, w_up, w_down):
+    )(outgoing, nearby, mine, kv, gate_w, up_w, down_w, mix)
+
+
+def expert_part(kv, moe_rows, moe_gain, routes, route_weights, w_gate, w_up, w_down):
     experts = lax.axis_size("ep")
     tp_count = lax.axis_size("tp")
     me = lax.axis_index("ep")
@@ -365,7 +406,7 @@
     mix = jnp.where(
         own_places.T[:, :, None] == slot_iota[None, None, :], weight_of.T[:, :, None], 0.0
     )
-    return run_experts(outgoing, nearby, mine, w_gate[0], w_up[0], w_down[0], mix)
+    return run_experts(outgoing, nearby, mine, kv, w_gate[0], w_up[0], w_down[0], mix)
 
 
 def local(
@@ -399,9 +440,17 @@
     start_acc = jnp.zeros((positions, kv_heads, per_key, 2, value_dim), jnp.float32)
     carry = (start_max, start_total, start_acc)
     both = jnp.concatenate([keys, values], axis=2)
-    gathered = lax.all_gather(both, "ep", axis=0, tiled=True)
-    moe_out = expert_part(moe_rows, moe_gain, routes, route_weights, w_gate, w_up, w_down)
-    gathered, moe_out = lax.optimization_barrier((gathered, moe_out))
+    moe_out, gathered = expert_part(
+        both.reshape(positions, -1),
+        moe_rows,
+        moe_gain,
+        routes,
+        route_weights,
+        w_gate,
+        w_up,
+        w_down,
+    )
+    gathered = gathered.reshape(-1, kv_heads, both.shape[2])
     key_piece = gathered[:, :, : keys.shape[2]]
     value_piece = gathered[:, :, keys.shape[2] :]
     shard_count = key_piece.shape[0] // positions

time: 198 us -> 195 us (0.985)
  between operations: 14.3 us -> 0.95 us
  Pallas kernels: 143 us -> 154 us
    pallas_call x1, Pallas kernels: 143 us -> 154 us  [run_experts(): pl.pallas_call(functools.partial(expert_kernel, n), out_shape=(jax.ShapeD...]
  transfers between devices with their start and end apart: 2 -> 1, of which waited for: 1 -> 1; matrix products, arithmetic and copies ran while one was open for 5% -> 0% of each run, Pallas kernels for 73% -> 0%
where the time goes in v4:
time: 195 us
  Pallas kernels  154 us (79%)
  other arithmetic  13.3 us (7%)
  matrix products  11.6 us (6%)
  local copies, waits for them, and re-layouts  5.56 us (3%)
  waiting for transfers between devices  4.57 us (2%)
  starting transfers between devices  3.33 us (2%)
    pallas_call x1, Pallas kernels, run_experts(): pl.pallas_call(functools.partial(expert_kernel, n), out_shape=(jax.ShapeD...  154 us
    all_to_all x1, waiting for transfers between devices, local(): lax.all_to_all(attn_rows.reshape(positions, q_heads, value_dim), 'tp', sp...  4.57 us
  transfers between devices with their start and end apart: 1, of which 1 were waited for; matrix products, arithmetic and copies ran while one was open for 0% of the time, Pallas kernels for 0%

profile of v4, /device:TPU:16, one launch (start us, length us, event | category | flops | bytes accessed | tf_op | source)
XLA Modules:
  0.0 194.8 jit_solution(17685315207769105349)
XLA Ops:
  0.7 0.5 iota_multiply_fusion
  1.2 0.7 xor_bitcast_fusion
  2.1 2.1 %fusion.23 = f32[512]{0:T(512)S(1)} fusion(bf16[512,2048]{1,0:T(8,128)(2,1)} %param.23), kind=kLoop, calls=%fused_computation.28 | loop fusion | flops 3145216 | bytes 2099200 | tf_op jit(solution)/shard_map/reduce_sum | solution.py:15
  4.3 2.1 %fusion.25 = bf16[512,2048]{1,0:T(8,128)(2,1)S(1)} fusion(bf16[512,2048]{1,0:T(8,128)(2,1)} %param.23, f32[2048]{0:T(1024)} %param.24, f32[512]{0:T(512)S(1)} %add_rsqrt_fusion.1), kind=kLoop, calls=%fused_computation.30 | loop fusion | flops 4194304 | bytes 4204544 | tf_op jit(solution)/shard_map/convert_element_type | solution.py:368
  6.4 2.0 %convolution_convert_fusion = bf16[512,2048]{1,0:T(8,128)(2,1)} fusion(pred[512,128]{1,0:T(32,128)(4,1)S(1)} %bitcast.142, bf16[4,128,2048]{2,1,0:T(8,128)(2,1)S(1)} %bitcast.132, s32[]{:T(128)S(6)} %select_n.45), kind=kOutput, calls=%fused_computation.31 | convolution fusion | flops 269484032 | bytes 2686980 | tf_op jit(solution)/shard_map/dot_general | solution.py:395
  8.5 1.4 convolution_convert_fusion.2
  9.9 1.1 fusion.32.mix_ref
  11.0 1.4 convolution_convert_fusion.1.mine_ref
  12.4 0.7 maximum_bitcast_fusion.kv_ref
  13.1 154.1 %shard_map.140 = (bf16[128,2048]{1,0:T(8,128)(2,1)}, bf16[8,256,256]{2,1,0:T(8,128)(2,1)}) custom-call(bf16[8,64,2048]{2,1,0:T(8,128)(2,1)} %bitcast.135, bf16[4,64,2048]{2,1,0:T(8,128)(2,1)} %bitcast.138, bf16[4,64,2048]{2,1,0:T(8,128)(2,1)} %convolution_convert_fusion.1.mine_ref, bf16[256,256]{1,0:T(8,128)(2,1)} %maximum_bitcast_fusion.kv_ref, ...), custom_call_target="tpu_custom_call" | custom-call | flops 257698037760 | bytes 16777216 | tf_op jit(solution)/shard_map/pallas_call | solution.py:329
  167.3 1.3 fusion.47
  169.0 0.7 copy.79
  170.2 9.3 %while.15 = (s32[]{:T(128)}, f32[256,1,2,2]{0,2,3,1:T(2,128)S(1)}, f32[256,1,2,2]{0,2,3,1:T(2,128)S(1)}, f32[256,1,2,2,128]{0,4,3,2,1:T(8,128)S(1)}, s32[2]{0:T(...) while((s32[]{:T(128)}, f32[256,1,2,2]{0,2,3,1:T(2,128)S(1)}, ...), condition=%wide.region_8.9_spmd.clone, body=%wide.region_3.8_spmd.clone.sunk | while | flops 411570432 | bytes 15155487 | solution.py:498
  170.3 0.6 dynamic_slice.77
  171.5 3.4 %conditional.3 = ((f32[256,1,2,2]{0,2,3,1:T(2,128)S(1)}, f32[256,1,2,2]{0,2,3,1:T(2,128)S(1)}, f32[256,1,2,2,128]{0,4,3,2,1:T(8,128)S(1)})) conditional(s32[]{:T(128)} %convert_element_type.76, (f32[256,1,2,2]{0,2,3,1:T(2,128)S(1)}, f32[256,1,2,2]{0,2,3,1:T(2,128)S(1)}, f32[256,1,2,2,128]{0,4,3,2,1:T(8,128)S(1)}) %tuple.51, (s32[]{:T(128)}, ...), branch_computations={%region_4.4_spmd, %region_5.7_spmd} | conditional | flops 411570432 | bytes 15154224 | solution.py:496
  171.5 0.6 iota_add_fusion
  172.4 0.9 fusion.4
  173.3 1.0 fusion.5
  174.3 0.5 fusion.11
  174.9 0.6 dynamic_slice.77
  176.1 3.4 %conditional.3 = ((f32[256,1,2,2]{0,2,3,1:T(2,128)S(1)}, f32[256,1,2,2]{0,2,3,1:T(2,128)S(1)}, f32[256,1,2,2,128]{0,4,3,2,1:T(8,128)S(1)})) conditional(s32[]{:T(128)} %convert_element_type.76, (f32[256,1,2,2]{0,2,3,1:T(2,128)S(1)}, f32[256,1,2,2]{0,2,3,1:T(2,128)S(1)}, f32[256,1,2,2,128]{0,4,3,2,1:T(8,128)S(1)}) %tuple.51, (s32[]{:T(128)}, ...), branch_computations={%region_4.4_spmd, %region_5.7_spmd} | conditional | flops 411570432 | bytes 15154224 | solution.py:496
  176.1 0.6 iota_add_fusion
  177.0 0.9 fusion.4
  177.9 1.0 fusion.5
  178.9 0.5 fusion.11
  179.9 0.7 broadcast_divide_fusion
  180.7 0.4 fusion.35
  181.1 1.0 fusion.39
  182.1 3.3 %all-to-all-start = ((bf16[256,2,128]{2,1,0:T(2,128)(2,1)}), bf16[256,2,128]{2,1,0:T(2,128)(2,1)S(1)}, u32[]{:S(2)}, u32[]{:S(2)}) async-start(bf16[256,2,128]{2,1,0:T(2,128)(2,1)} %fusion.39), calls=%async_computation | async-start | bytes 262144 | tf_op jit(solution)/shard_map/all_to_all | solution.py:508
  185.5 4.6 %all-to-all-done = bf16[256,2,128]{2,1,0:T(2,128)(2,1)S(1)} async-done(((bf16[256,2,128]{2,1,0:T(2,128)(2,1)}), bf16[256,2,128]{2,1,0:T(2,128)(2,1)S(1)}, u32[]{:S(2)}, u32[]{:S(2)}) %all-to-all-start) | async-done | bytes 131104 | tf_op jit(solution)/shard_map/all_to_all | solution.py:508
  190.3 3.7 %convolution_convert_fusion.3 = bf16[64,2048]{1,0:T(8,128)(2,1)} fusion(bf16[64,1024]{1,0:T(8,128)(2,1)S(1)} %reshape.264, bf16[1024,2048]{1,0:T(8,128)(2,1)} %param.22), kind=kOutput, calls=%fused_computation.34 | convolution fusion | flops 268566528 | bytes 4587520 | tf_op jit(solution)/shard_map/dot_general | solution.py:515
  194.0 0.8 copy.126
  (53 shorter events, 2.2 us)
Async XLA Ops:
  0.6 9.3 %copy-start = (f32[512,2]{0,1:T(2,128)S(1)}, f32[512,2]{0,1:T(2,128)}, u32[]{:S(2)}) copy-start(f32[512,2]{0,1:T(2,128)} %param.26) | copy-start | bytes 12292
  6.4 6.0 %copy-start.3 = (bf16[256,1,128]{2,0,1:T(8,128)(2,1)S(1)}, bf16[256,1,128]{2,0,1:T(8,128)(2,1)}, u32[]{:S(2)}) copy-start(bf16[256,1,128]{2,0,1:T(8,128)(2,1)} %param.19) | copy-start | bytes 196612
  6.4 6.0 %copy-start.4 = (bf16[256,1,128]{2,0,1:T(8,128)(2,1)S(1)}, bf16[256,1,128]{2,0,1:T(8,128)(2,1)}, u32[]{:S(2)}) copy-start(bf16[256,1,128]{2,0,1:T(8,128)(2,1)} %param.18) | copy-start | bytes 196612
  167.3 2.7 %copy-start.2 = (bf16[256,2,128]{2,1,0:T(2,128)(2,1)S(1)}, bf16[256,2,128]{2,1,0:T(2,128)(2,1)}, u32[]{:S(2)}) copy-start(bf16[256,2,128]{2,1,0:T(2,128)(2,1)} %param.17) | copy-start | bytes 393220
  167.3 2.9 %copy-start.7 = (s32[2]{0:T(128)S(1)}, s32[2]{0:T(128)}, u32[]{:S(2)}) copy-start(s32[2]{0:T(128)} %iota_multiply_fusion) | copy-start | bytes 28
  170.2 10.4 %copy-start.5 = (f32[2]{0:T(128)S(1)}, f32[2]{0:T(128)}, u32[]{:S(2)}) copy-start(f32[2]{0:T(128)} %param.20) | copy-start | bytes 28
  170.2 10.9 %copy-start.6 = (f32[128]{0:T(128)S(1)}, f32[128]{0:T(128)}, u32[]{:S(2)}) copy-start(f32[128]{0:T(128)} %param.21) | copy-start | bytes 1540
  179.9 14.1 %copy-start.1 = (bf16[128,2048]{1,0:T(8,128)(2,1)S(1)}, bf16[128,2048]{1,0:T(8,128)(2,1)}, u32[]{:S(2)}) copy-start(bf16[128,2048]{1,0:T(8,128)(2,1)} %get-tuple-element.364) | copy-start | bytes 1572868
  182.1 7.9 %all-to-all-start = ((bf16[256,2,128]{2,1,0:T(2,128)(2,1)}), bf16[256,2,128]{2,1,0:T(2,128)(2,1)S(1)}, u32[]{:S(2)}, u32[]{:S(2)}) async-start(bf16[256,2,128]{2,1,0:T(2,128)(2,1)} %fusion.39), calls=%async_computation | async-start | bytes 262144 | tf_op jit(solution)/shard_map/all_to_all | solution.py:508
